TPU v7x, 32 devices: a whole 2x2x4 slice. The times are simulated.
32 devices in a mesh: grp: 2 (over y), sp: 4 (over z), tp: 4 (over x, core).
Axes of the slice: x: 2, y: 2, z: 4, core: 2. Of those that a mesh axis runs over, the one named last changes fastest.
Arguments:
- tokens: bfloat16 [4096, 4096], P(('grp', 'sp', 'tp')), parts along dimension 0, may hold values from -6 to 6
- norm_gain: float32 [4096], replicated, may hold values from 0.1 to 1.9
- query_diff: bfloat16 [4096, 2048], P('sp', 'tp'), may hold values from -1.25 to 1.25
- key_diff: bfloat16 [4096, 2048], P('sp', 'tp'), may hold values from -1.25 to 1.25
- value_diff: bfloat16 [4096, 2048], P('sp', 'tp'), may hold values from -0.09375 to 0.09375
- lam: float32 [8], P('tp'), may hold values from 0.3 to 0.8
- output_norm_gain: float32 [256], replicated, may hold values from 0.1 to 1.9
- query_win: bfloat16 [4096, 2048], P('sp', 'tp'), may hold values from -1.25 to 1.25
- keyval_win: bfloat16 [4, 4096, 256], P(None, 'sp'), may hold values from -1.25 to 1.25
- sink: float32 [16], P('tp'), may hold values from 4 to 7
- proj_diff: bfloat16 [2048, 4096], P('tp'), may hold values from -0.125 to 0.125
- proj_win: bfloat16 [2048, 4096], P('tp'), may hold values from -0.79296875 to 0.79296875
Outputs:
- mixed: bfloat16 [4096, 4096], P(('grp', 'sp', 'tp')), parts along dimension 0
There are 2 independent parts, one for each index of `grp`. A program takes and returns all parts, laid end to end along the dimension named above; an argument that names none is the same for every part. Nothing has to cross between parts.
All inputs are finite; a program needn't handle non-finite values.
Results may differ from a plain program's by a relative error of at most 0.015.
Values may be sent and summed in bfloat16 or wider, within the bound.
A program may use at most 128 MiB of HBM per device.

v0:
```python
import functools
import math

import jax
import jax.numpy as jnp
from jax import lax
from jax.experimental import pallas as pl
from jax.experimental.pallas import tpu as pltpu
from jax.sharding import PartitionSpec as P


HEAD = 128
WIN_HEADS = 16
KV_HEADS = 4
WINDOW = 128
VDIM = 256


EPS = 1e-06


def padded_2(x, sides, width):
    for axis, dim in sides:
        devices, length = (lax.axis_size(axis), x.shape[dim])
        up = [(i, (i + 1) % devices) for i in range(devices - 1)]
        down = [(j, i) for i, j in up]
        last = lax.slice_in_dim(x, length - width, length, axis=dim)
        first = lax.slice_in_dim(x, 0, width, axis=dim)
        before = lax.ppermute(last, axis, up)
        after = lax.ppermute(first, axis, down)
        x = jnp.concatenate([before, x, after], axis=dim)
    return x


def root_mean_square_rows(values, gain):
    return values * lax.rsqrt(jnp.mean(values * values, axis=-1, keepdims=True) + EPS) * gain


def shifted(x, axis, by):
    n = lax.axis_size(axis)
    return lax.ppermute(x, axis, [(i, (i + by) % n) for i in range(n)])


def shift_chip(x, by):
    n = lax.axis_size("tp")
    return lax.ppermute(x, "tp", [(i, (i + 2 * by) % n) for i in range(n)])


def swap_core(x):
    n = lax.axis_size("tp")
    return lax.ppermute(x, "tp", [(i, i ^ 1) for i in range(n)])


def gather_tp(x, axis):
    tp = lax.axis_size("tp")
    chips = tp // 2
    me = lax.axis_index("tp")
    mine = [x] + [shift_chip(x, r) for r in range(1, chips)]
    theirs = [swap_core(piece) for piece in mine]
    out = jnp.zeros(x.shape[:axis] + (tp,) + x.shape[axis:], x.dtype)
    for r in range(chips):
        at = (me - 2 * r) % tp
        out = lax.dynamic_update_slice_in_dim(out, jnp.expand_dims(mine[r], axis), at, axis)
        out = lax.dynamic_update_slice_in_dim(out, jnp.expand_dims(theirs[r], axis), at ^ 1, axis)
    return out


def scatter_tp(x):
    tp = lax.axis_size("tp")
    chips = tp // 2
    me = lax.axis_index("tp")
    core, chip = me % 2, me // 2
    x = x.reshape(chips, 2, x.shape[0] // tp, x.shape[1])
    away = lax.dynamic_index_in_dim(x, 1 - core, 1, keepdims=False).astype(jnp.bfloat16)
    keep = lax.dynamic_index_in_dim(x, core, 1, keepdims=False)
    both = keep + swap_core(away).astype(jnp.float32)
    total = lax.dynamic_index_in_dim(both, chip, 0, keepdims=False)
    for r in range(1, chips):
        sent = lax.dynamic_index_in_dim(both, (chip + r) % chips, 0, keepdims=False)
        total = total + shift_chip(sent.astype(jnp.bfloat16), r).astype(jnp.float32)
    return total.astype(jnp.bfloat16)


def diff_kernel(lam_ref, q_ref, k_ref, v_ref, gain_ref, o_ref):
    factor = HEAD ** (-0.5) * math.log2(math.e)
    maps = []
    for m in range(2):
        cols = slice(m * HEAD, (m + 1) * HEAD)
        scores = lax.dot_general(
            q_ref[:, cols], k_ref[:, cols], (((1,), (1,)), ((), ())),
            preferred_element_type=jnp.float32,
        )
        top = jnp.max(scores, axis=-1, keepdims=True)
        expo = jnp.exp2((scores - top) * factor)
        total = jnp.sum(expo, axis=-1, keepdims=True)
        out = jnp.dot(expo.astype(jnp.bfloat16), v_ref[...], preferred_element_type=jnp.float32)
        maps.append(out / total)
    d = maps[0] - lam_ref[pl.program_id(0)] * maps[1]
    d = d * lax.rsqrt(jnp.mean(d * d, axis=-1, keepdims=True) + EPS) * gain_ref[...]
    o_ref[...] = d.astype(jnp.bfloat16)


def diff_attention(q, kv, lam, gain):
    tok, rows, heads = q.shape[0], kv.shape[0], lam.shape[0]
    tile = math.gcd(tok, max(128, 524288 // rows))
    return pl.pallas_call(
        diff_kernel,
        grid=(heads, tok // tile),
        in_specs=[
            pl.BlockSpec(memory_space=pltpu.SMEM),
            pl.BlockSpec((tile, 2 * HEAD), lambda h, i: (i, h)),
            pl.BlockSpec((rows, 2 * HEAD), lambda h, i: (0, h)),
            pl.BlockSpec((rows, VDIM), lambda h, i: (0, heads + h)),
            pl.BlockSpec((1, VDIM), lambda h, i: (0, 0)),
        ],
        out_specs=pl.BlockSpec((tile, VDIM), lambda h, i: (i, h)),
        out_shape=jax.ShapeDtypeStruct((tok, heads * VDIM), jnp.bfloat16),
        cost_estimate=pl.CostEstimate(
            flops=heads * tok * rows * 2 * 2 * (HEAD + VDIM),
            bytes_accessed=2 * (q.size * 2 + kv.size),
            transcendentals=heads * 2 * tok * rows,
        ),
    )(lam, q, kv, kv, gain.reshape(1, VDIM))


def general_body(
    tokens,
    norm_gain,
    query_diff,
    key_diff,
    value_diff,
    lam,
    output_norm_gain,
    query_win,
    keyval_win,
    sink,
    proj_diff,
    proj_win,
):
    bf16, f32 = jnp.bfloat16, jnp.float32
    normed = root_mean_square_rows(tokens.astype(f32), norm_gain).astype(bf16)
    heads_win = sink.shape[0]
    group = WIN_HEADS // KV_HEADS
    n = lax.axis_size("sp")
    me = lax.axis_index("sp")
    parts = lax.axis_size("grp")
    part = lax.axis_index("grp")
    local, width = normed.shape
    depth = width // n
    tok = local * lax.axis_size("tp")

    slabs = normed.reshape(local, n, depth)
    across = jnp.zeros((n, local, depth), bf16)
    own = lax.dynamic_index_in_dim(slabs, me, 1, keepdims=True)
    across = lax.dynamic_update_slice_in_dim(across, jnp.swapaxes(own, 0, 1), me, 0)
    for r in range(1, n):
        sent = lax.dynamic_index_in_dim(slabs, (me + r) % n, 1, keepdims=False)
        got = shifted(sent, "sp", r)
        across = lax.dynamic_update_slice_in_dim(across, got[None], (me - r) % n, 0)

    kv_index = lax.axis_index("tp") * heads_win // group
    kv_local = lax.dynamic_index_in_dim(keyval_win, kv_index, 0, keepdims=False)
    stacked = jnp.concatenate([query_diff, query_win, kv_local], axis=1)
    share = stacked.shape[1] // parts
    half = lax.dynamic_slice_in_dim(stacked, part * share, share, axis=1)
    across, half = lax.optimization_barrier((across, half))

    pieces = [shifted(half, "sp", r) for r in range(1, n)]
    all_rows = gather_tp(across, 1).reshape(n * tok, depth)
    rows_all = gather_tp(normed, 0).reshape(tok, width)
    kv_part = jnp.concatenate(
        [
            jnp.dot(all_rows, key_diff, preferred_element_type=f32).astype(bf16),
            jnp.dot(all_rows, value_diff, preferred_element_type=f32).astype(bf16),
        ],
        axis=1,
    )
    kv = lax.psum_scatter(kv_part, "sp", scatter_dimension=0, tiled=True)
    kv = lax.all_gather(kv, "sp", axis=0, tiled=True)

    own_rows = lax.dynamic_slice_in_dim(rows_all, me * depth, depth, axis=1)
    own_sum = jnp.dot(own_rows, stacked, preferred_element_type=f32)
    sums = [jnp.zeros((tok, share), f32) for _ in range(parts)]
    for r in range(1, n):
        piece = pieces[r - 1]
        rows = lax.dynamic_slice_in_dim(rows_all, (me - r) % n * depth, depth, axis=1)
        for j in range(parts):
            block = piece if j == 0 else shifted(piece, "grp", j)
            sums[j] = sums[j] + jnp.dot(rows, block, preferred_element_type=f32)
    ordered = jnp.stack(sums)
    ordered = jnp.concatenate(
        [
            lax.dynamic_index_in_dim(ordered, (part - b) % parts, 0, keepdims=False)
            for b in range(parts)
        ],
        axis=1,
    )
    projected = (own_sum + ordered).astype(bf16)
    first = query_diff.shape[1]
    second = first + query_win.shape[1]
    q_diff, q_win, kv_win = projected[:, :first], projected[:, first:second], projected[:, second:]
    scale = HEAD ** (-0.5)
    padded = padded_2(kv_win, (("sp", 0),), WINDOW)
    nblocks = tok // WINDOW
    blocks = padded.reshape(nblocks + 2, WINDOW, 2 * HEAD)
    band = jnp.concatenate([blocks[:-2], blocks[1:-1], blocks[2:]], axis=1)
    q_blocks = q_win.reshape(nblocks, WINDOW, heads_win, HEAD)
    scores = (
        jnp.einsum("nqhd,nkd->nhqk", q_blocks, band[..., :HEAD], preferred_element_type=jnp.float32)
        * scale
    )
    q_index = jnp.arange(WINDOW)
    k_index = jnp.arange(3 * WINDOW)
    relative = k_index[None, :] - WINDOW - q_index[:, None]
    first_key = lax.axis_index("sp") * tok - WINDOW
    key_pos = first_key + jnp.arange(nblocks)[:, None] * WINDOW + k_index[None, :]
    inside = (key_pos >= 0) & (key_pos < tok * lax.axis_size("sp"))
    valid = (jnp.abs(relative) <= WINDOW)[None] & inside[:, None, :]
    scores = jnp.where(valid[:, None], scores, -jnp.inf)
    sink_logit = sink[None, :, None, None]
    top_win = jnp.maximum(jnp.max(scores, axis=-1, keepdims=True), sink_logit)
    expo = jnp.exp(scores - top_win)
    weights = expo / (jnp.sum(expo, axis=-1, keepdims=True) + jnp.exp(sink_logit - top_win))
    y_win = jnp.einsum(
        "nhqk,nkd->nqhd",
        weights.astype(jnp.bfloat16),
        band[..., HEAD:],
        preferred_element_type=jnp.float32,
    ).astype(jnp.bfloat16)
    y_win = y_win.reshape(tok, heads_win * HEAD)
    summed = jnp.dot(y_win, proj_win, preferred_element_type=jnp.float32)
    differential_output = diff_attention(q_diff, kv, lam, output_norm_gain)
    summed = summed + jnp.dot(differential_output, proj_diff, preferred_element_type=jnp.float32)
    return scatter_tp(summed)


MESH = pl.DeviceIdType.MESH
CHUNKS = 4
LANES = 128
MATS = 5


def remote(src, dst, send, recv, device):
    return pltpu.make_async_remote_copy(
        src_ref=src, dst_ref=dst, send_sem=send, recv_sem=recv, device_id=device, device_id_type=MESH
    )


def place():
    g, z, t = lax.axis_index("grp"), lax.axis_index("sp"), lax.axis_index("tp")
    x, c = t // 2, t % 2
    return g, z, t, x, c, 2 * (1 - x) + c, 2 * x + 1 - c


def greet(devices):
    barrier = pltpu.get_barrier_semaphore()
    for device in devices:
        pl.semaphore_signal(barrier, inc=1, device_id=device, device_id_type=MESH)
    pl.semaphore_wait(barrier, len(devices))


def project_kernel(
    n, held, tok_ref, gain_ref, qd, qw, kd, vd, kvw, pd, pw, scal_ref,
    res_ref, opd, opw, oscal_ref,
    rows_ref, w_ref, zs, zr, xs, xr, cs, cr, ws, wr, ys, yr, own_sem, rs, rr, ps, pr, scal_s, scal_r,
):
    g, z, t, x, c, t_x, t_c = place()
    local, _ = tok_ref.shape
    part = local // CHUNKS
    depth = qd.shape[0]
    half = depth // 2
    group = WIN_HEADS // KV_HEADS
    mats = (qd, qw, kd, vd, kvw)
    core = (g, z, t_c)

    def block(zz, h, tt):
        return rows_ref.at[zz, h, pl.ds(pl.multiple_of(tt * part, part), part)]

    for h in range(CHUNKS):
        v = tok_ref[h * part:(h + 1) * part, :].astype(jnp.float32)
        v = v * lax.rsqrt(jnp.mean(v * v, axis=-1, keepdims=True) + EPS) * gain_ref[...]
        rows_ref[z, h, pl.ds(pl.multiple_of(t * part, part), part), :] = v.astype(jnp.bfloat16)
    oscal_ref[c] = scal_ref[...]

    greet(
        [(g, lax.rem(z + i // 2, n), 2 * x + (c + i % 2) % 2) for i in range(1, 2 * n)]
        + [(g, z, t_x), (1 - g, z, t)]
    )

    def w_own(zz, yy, m):
        return w_ref.at[pl.ds(pl.multiple_of(zz * depth + yy * half, half), half), m * LANES:(m + 1) * LANES]

    def w_copy(i, cc, m, remote_half):
        dz = c * held + i
        lanes = slice((2 * i + cc) * LANES, (2 * i + cc + 1) * LANES)
        if m == MATS - 1:
            source = kvw.at[(2 * (x * n + dz)) // group]
            lanes = slice(cc * LANES, (cc + 1) * LANES)
        else:
            source = mats[m]
        if remote_half:
            return remote(
                source.at[pl.ds(pl.multiple_of(g * half, half), half), lanes], w_own(z, g, m),
                ws.at[i, cc, m], wr.at[z, m], (g, dz, 2 * x + cc),
            )
        target = w_ref.at[pl.ds(pl.multiple_of(z * depth, depth), depth), m * LANES:(m + 1) * LANES]
        return source.at[:, lanes], target

    def each_weight(act):
        for m in range(MATS):
            for i in range(held):
                for cc in range(2):
                    act(m, i, cc)

    def w_start(m, i, cc):
        dz = c * held + i

        @pl.when(dz != z)
        def _():
            w_copy(i, cc, m, True).start()

    def w_start_own(m, i, cc):
        dz = c * held + i
        source, target = w_copy(i, cc, m, False)

        @pl.when((dz == z) & (cc == c))
        def _():
            pltpu.make_async_copy(source, target, own_sem.at[m]).start()

        @pl.when((dz == z) & (cc != c))
        def _():
            remote(source, target, ws.at[i, cc, m], own_sem.at[m], core).start()

    def w_wait_send(m, i, cc):
        dz = c * held + i
        source, target = w_copy(i, cc, m, False)

        @pl.when(dz != z)
        def _():
            w_copy(i, cc, m, True).wait_send()

        @pl.when((dz == z) & (cc != c))
        def _():
            remote(source, target, ws.at[i, cc, m], own_sem.at[m], core).wait_send()

    def z_copy(way, k, h):
        zz = z - k if way == 0 else z + k
        to = z + 1 if way == 0 else z - 1
        return remote(block(zz, h, t), block(zz, h, t), zs.at[way, k, h], zr.at[way, k + 1, h], (g, to, t))

    def z_wait(way, k, h):
        zz = z - k if way == 0 else z + k
        remote(block(zz, h, t), block(zz, h, t), zs.at[way, k, h], zr.at[way, k, h], core).wait_recv()

    def x_copy(zz, h):
        return remote(block(zz, h, t), block(zz, h, t), xs.at[zz, h], xr.at[zz, h], (g, z, t_x))

    def c_copy(zz, xx, h):
        tt = 2 * xx + c
        return remote(block(zz, h, tt), block(zz, h, tt), cs.at[zz, xx, h], cr.at[zz, xx, h], core)

    def y_copy(zz, m):
        return remote(w_own(zz, g, m), w_own(zz, g, m), ys.at[zz, m], yr.at[zz, m], (1 - g, z, t))

    each_weight(w_start)
    for h in range(CHUNKS):
        @pl.when(z < n - 1)
        def _(h=h):
            z_copy(0, 0, h).start()

        @pl.when(z > 0)
        def _(h=h):
            z_copy(1, 0, h).start()

        x_copy(z, h).start()
        c_copy(z, x, h).start()
    scal_copy = remote(scal_ref, oscal_ref.at[c], scal_s, scal_r, core)
    scal_copy.start()
    each_weight(w_start_own)
    proj_copies = [remote(pd, opd, ps.at[0], pr.at[0], core), remote(pw, opw, ps.at[1], pr.at[1], core)]
    for copy in proj_copies:
        copy.start()

    def sides(k, act):
        @pl.when(z - k >= 0)
        def _():
            act(z - k, 0)

        @pl.when((z + k < n) & (k > 0))
        def _():
            act(z + k, 1)

    for d in range(1, n):
        def forward(zz, way):
            def one(m):
                remote(w_own(zz, g, m), w_own(zz, g, m), ys.at[zz, m], wr.at[zz, m], core).wait_recv()
                y_copy(zz, m).start()

            for m in range(MATS):
                one(m)

        sides(d, forward)

    def stage_a(e):
        k, h = e // CHUNKS, e % CHUNKS

        def act(zz, way):
            z_wait(way, k, h)

            @pl.when(z < n - 1 if way == 0 else z > 0)
            def _():
                z_copy(way, k, h).start()

            x_copy(zz, h).start()
            c_copy(zz, x, h).start()

        sides(k, act)

    def stage_b(e):
        k, h = e // CHUNKS, e % CHUNKS

        def act(zz, way):
            x_copy(zz, h).wait_recv()
            c_copy(zz, 1 - x, h).start()

        sides(k, act)

    def stage_c(e, carry):
        k, h = e // CHUNKS, e % CHUNKS

        def act(zz, way):
            for xx in range(2):
                c_copy(zz, xx, h).wait_recv()
            res_ref[c, zz, h] = jnp.dot(
                rows_ref[zz, h], w_ref[...], preferred_element_type=jnp.float32
            ).astype(jnp.bfloat16)

        sides(k, act)
        return carry

    def r_copies(zz, h):
        copies = [remote(
            res_ref.at[c, zz, h, :, 2 * LANES:], res_ref.at[c, zz, h, :, 2 * LANES:],
            rs.at[zz, h, 0], rr.at[zz, h, 0], core,
        )]
        for xx in range(2):
            at = pl.ds(pl.multiple_of((2 * xx + 1 - c) * part, part), part)
            copies.append(remote(
                res_ref.at[c, zz, h, at, :2 * LANES], res_ref.at[c, zz, h, at, :2 * LANES],
                rs.at[zz, h, 1 + xx], rr.at[zz, h, 1 + xx], core,
            ))
        return copies

    def stage_d(e, carry):
        k, h = e // CHUNKS, e % CHUNKS

        def act(zz, way):
            for copy in r_copies(zz, h):
                copy.start()

        sides(k, act)
        return carry

    for e in range(CHUNKS - 1):
        stage_b(e)

    last = n * CHUNKS

    def upto(e):
        return jnp.maximum(jnp.minimum(2 * (e - 2 * CHUNKS + 1), e - 1), 0)

    def weights_ready():
        for m in range(MATS):
            source, target = w_copy(0, 0, m, False)
            pltpu.make_async_copy(source, target, own_sem.at[m]).wait()
        for d in range(1, n):
            def arrived(zz, way):
                for m in range(MATS):
                    remote(w_own(zz, 1 - g, m), w_own(zz, 1 - g, m), ys.at[zz, m], yr.at[zz, m], core).wait_recv()

            sides(d, arrived)

    def step(e, carry):
        @pl.when(e < last)
        def _():
            stage_a(e)

        @pl.when(e < last + 1)
        def _():
            stage_b(e - 1)

        pl.when(e == 2 * CHUNKS)(weights_ready)
        lax.fori_loop(upto(e - 2), upto(e - 1), stage_d, 0)
        lax.fori_loop(upto(e - 1), upto(e), stage_c, 0)
        return carry

    lax.fori_loop(CHUNKS, last + 2, step, 0)
    for copy in proj_copies + [scal_copy]:
        copy.wait()
    each_weight(w_wait_send)
    lax.fori_loop(upto(last), upto(last + 1), stage_d, 0)

    def drain(e, carry):
        k, h = e // CHUNKS, e % CHUNKS

        def act(zz, way):
            @pl.when(z < n - 1 if way == 0 else z > 0)
            def _():
                z_copy(way, k, h).wait_send()

            x_copy(zz, h).wait_send()
            for xx in range(2):
                c_copy(zz, xx, h).wait_send()
            for copy in r_copies(zz, h):
                copy.wait()

        sides(k, act)

        @pl.when((k == 0) & (z > 0))
        def _():
            z_copy(1, 0, h).wait_send()

        return carry

    lax.fori_loop(0, last, drain, 0)
    for d in range(1, n):
        def sent(zz, way):
            for m in range(MATS):
                y_copy(zz, m).wait_send()

        sides(d, sent)


def project(n, tokens, norm_gain, query_diff, query_win, key_diff, value_diff, keyval_win, proj_diff, proj_win, scal):
    local, width = tokens.shape
    held = n // 2
    dma = pltpu.SemaphoreType.DMA
    whole = pl.BlockSpec(memory_space=pltpu.VMEM)
    far = pl.BlockSpec(memory_space=pl.ANY)
    cols = MATS * LANES
    tok = 4 * local * n
    return pl.pallas_call(
        functools.partial(project_kernel, n, held),
        in_specs=[whole, whole] + [far] * 7 + [whole],
        out_specs=[whole, far, far, whole],
        out_shape=[
            jax.ShapeDtypeStruct((2, n, CHUNKS, 4 * local // CHUNKS, cols), jnp.bfloat16),
            jax.ShapeDtypeStruct(proj_diff.shape, proj_diff.dtype),
            jax.ShapeDtypeStruct(proj_win.shape, proj_win.dtype),
            jax.ShapeDtypeStruct((2,) + scal.shape, scal.dtype),
        ],
        scratch_shapes=[
            pltpu.VMEM((n, CHUNKS, 4 * local // CHUNKS, width), jnp.bfloat16),
            pltpu.VMEM((width, cols), jnp.bfloat16),
            dma((2, n, CHUNKS)), dma((2, n + 1, CHUNKS)),
            dma((n, CHUNKS)), dma((n, CHUNKS)),
            dma((n, 2, CHUNKS)), dma((n, 2, CHUNKS)),
            dma((held, 2, MATS)), dma((n, MATS)),
            dma((n, MATS)), dma((n, MATS)), dma((MATS,)),
            dma((n, CHUNKS, 3)), dma((n, CHUNKS, 3)),
            dma((2,)), dma((2,)), dma, dma,
        ],
        compiler_params=pltpu.CompilerParams(
            collective_id=0, has_side_effects=True, vmem_limit_bytes=52 << 20
        ),
        cost_estimate=pl.CostEstimate(
            flops=2 * tok * width * cols, bytes_accessed=2 * width * (tok + cols), transcendentals=0
        ),
    )(tokens, norm_gain.reshape(1, width), query_diff, query_win, key_diff, value_diff, keyval_win, proj_diff, proj_win, scal)


def attend_kernel(n, scal_ref, res_ref, gain_ref, y_ref, v_ref):
    z, t = lax.axis_index("sp"), lax.axis_index("tp")
    c = t % 2
    zz = pl.program_id(0)
    chunks, quad, _ = res_ref.shape[2:]
    part = quad // 4
    local = part * chunks
    rows = n * chunks * quad
    factor = HEAD ** (-0.5) * math.log2(math.e)
    f32, bf16 = jnp.float32, jnp.bfloat16

    @pl.when(zz == 0)
    def _():
        for i in range(2):
            v_ref[:, i * LANES:(i + 1) * LANES] = res_ref[i, :, :, :, 3 * LANES:4 * LANES].reshape(rows, LANES)

    def own(i, xx, m):
        at = pl.ds(pl.multiple_of((2 * xx + c) * part, part), part)
        return res_ref[i, zz, :, at, m * LANES:(m + 1) * LANES].reshape(local, LANES)

    maps = []
    for m in range(2):
        q = jnp.concatenate([own(m, xx, 0) for xx in range(2)], axis=0)
        keys = res_ref[m, :, :, :, 2 * LANES:3 * LANES].reshape(rows, LANES)
        scores = lax.dot_general(q, keys, (((1,), (1,)), ((), ())), preferred_element_type=f32)
        top = jnp.max(scores, axis=-1, keepdims=True)
        expo = jnp.exp2((scores - top) * factor)
        total = jnp.sum(expo, axis=-1, keepdims=True)
        out = jnp.dot(expo.astype(bf16), v_ref[...], preferred_element_type=f32)
        maps.append(out / total)
    lam = scal_ref[z // (n // 2), 0, z % (n // 2)]
    d = maps[0] - lam * maps[1]
    d = d * lax.rsqrt(jnp.mean(d * d, axis=-1, keepdims=True) + EPS) * gain_ref[...]
    y_ref[0, :, :, :VDIM] = d.astype(bf16).reshape(2, local, VDIM)

    held = n // 2
    r_index = lax.broadcasted_iota(jnp.int32, (2 * local, 3 * local), 0) % local
    k_index = lax.broadcasted_iota(jnp.int32, (2 * local, 3 * local), 1)
    near = jnp.abs(k_index - local - r_index) <= WINDOW
    first = lax.broadcasted_iota(jnp.int32, (2 * local, 1), 0) < local
    sinks = [scal_ref[z // held, 1, 2 * (z % held) + i] for i in range(2)]
    sink = jnp.where(first, sinks[0], sinks[1])
    for xx in range(2):
        b = 4 * zz + 2 * xx + c

        def banded(i):
            pieces = []
            for s in (-1, 0, 1):
                o = jnp.clip(b + s, 0, 4 * n - 1)
                at = pl.ds(pl.multiple_of(o % 4 * part, part), part)
                pieces.append(res_ref[i, o // 4, :, at, 4 * LANES:5 * LANES].reshape(local, LANES))
            return jnp.concatenate(pieces, axis=0)

        q = jnp.concatenate([own(i, xx, 1) for i in range(2)], axis=0)
        scores = lax.dot_general(
            q, banded(0), (((1,), (1,)), ((), ())), preferred_element_type=f32
        ) * HEAD ** (-0.5)
        spot = (b - 1) * local + k_index
        valid = near & (spot >= 0) & (spot < rows)
        scores = jnp.where(valid, scores, -jnp.inf)
        top = jnp.maximum(jnp.max(scores, axis=-1, keepdims=True), sink)
        expo = jnp.exp(scores - top)
        weights = expo / (jnp.sum(expo, axis=-1, keepdims=True) + jnp.exp(sink - top))
        out = jnp.dot(weights.astype(bf16), banded(1), preferred_element_type=f32).astype(bf16)
        for i in range(2):
            y_ref[0, xx, :, VDIM + i * LANES:VDIM + (i + 1) * LANES] = out[i * local:(i + 1) * local]


def attend(n, scal, res, gain):
    chunks, quad, _ = res.shape[2:]
    local = quad * chunks // 4
    rows = n * chunks * quad
    feats = VDIM + 2 * HEAD
    return pl.pallas_call(
        functools.partial(attend_kernel, n),
        grid=(n,),
        in_specs=[
            pl.BlockSpec(memory_space=pltpu.SMEM),
            pl.BlockSpec(memory_space=pltpu.VMEM),
            pl.BlockSpec(memory_space=pltpu.VMEM),
        ],
        out_specs=pl.BlockSpec((1, 2, local, feats), lambda i: (i, 0, 0, 0)),
        out_shape=jax.ShapeDtypeStruct((n, 2, local, feats), jnp.bfloat16),
        scratch_shapes=[pltpu.VMEM((rows, VDIM), jnp.bfloat16)],
        cost_estimate=pl.CostEstimate(
            flops=rows * rows * 2 * (HEAD + VDIM), bytes_accessed=2 * res.size, transcendentals=rows * rows
        ),
    )(scal, res, gain.reshape(1, VDIM))


def finish_kernel(
    n, y_ref, pd, pw, opd, opw, out_ref,
    got_ref, p_ref, mine_ref, away_ref, theirs_ref, ys, yr, load, ds, dr,
):
    g, z, t, x, c, t_x, _ = place()
    held = n // 2
    local, width = out_ref.shape
    steps = mine_ref.shape[0]
    wide = width // steps
    f32, bf16 = jnp.float32, jnp.bfloat16

    loads = []
    for i in range(held):
        for far, at, a, b in ((0, c, pd, pw), (1, 1 - c, opd, opw)):
            for j, ref in enumerate((a, b)):
                loads.append(pltpu.make_async_copy(
                    ref.at[i * VDIM:(i + 1) * VDIM], p_ref.at[at * held + i, j * VDIM:(j + 1) * VDIM],
                    load.at[i, far, j],
                ))
    for copy in loads:
        copy.start()

    greet([(g, lax.rem(z + i, n), t) for i in range(1, n)] + [(g, z, t_x)])

    def y_copy(zz, xx):
        return remote(y_ref.at[zz, xx], got_ref.at[z, xx], ys.at[zz, xx], yr.at[z, xx], (g, zz, t))

    def y_wait(zz, xx):
        return remote(got_ref.at[zz, xx], got_ref.at[zz, xx], ys.at[zz, xx], yr.at[zz, xx], (g, z, t_x))

    def others(act):
        for d in range(n - 1, 0, -1):
            pl.when(z - d >= 0)(functools.partial(act, z - d))
            pl.when(z + d < n)(functools.partial(act, z + d))

    for xx in (1 - x, x):
        others(lambda zz: y_copy(zz, xx).start())
    got_ref[z] = y_ref[z]
    for copy in loads:
        copy.wait()

    def product(j, xx):
        total = jnp.zeros((local, wide), f32)
        at = pl.ds(pl.multiple_of(j * wide, wide), wide)
        for zz in range(n):
            total = total + jnp.dot(got_ref[zz, xx], p_ref[zz, :, at], preferred_element_type=f32)
        return total

    def d_copy(j):
        return remote(away_ref.at[j], theirs_ref.at[j], ds.at[j], dr.at[j], (g, z, t_x))

    others(lambda zz: y_wait(zz, 1 - x).wait_recv())

    def send(j, carry):
        value = product(j, 1 - x).astype(bf16)

        @pl.when(j > 0)
        def _():
            d_copy(j - 1).start()

        away_ref[j] = value
        return carry

    lax.fori_loop(0, steps, send, 0)
    others(lambda zz: y_wait(zz, x).wait_recv())
    d_copy(steps - 1).start()

    def keep(j, carry):
        mine_ref[j] = product(j, x)
        return carry

    lax.fori_loop(0, steps, keep, 0)
    for j in range(steps):
        d_copy(j).wait_recv()
        out_ref[:, j * wide:(j + 1) * wide] = (mine_ref[j] + theirs_ref[j].astype(f32)).astype(bf16)
    for j in range(steps):
        d_copy(j).wait_send()
    for xx in (1 - x, x):
        others(lambda zz: y_copy(zz, xx).wait_send())


def finish(n, y, proj_diff, proj_win, other_diff, other_win):
    local, feats = y.shape[2:]
    width = proj_diff.shape[1]
    steps = 8
    dma = pltpu.SemaphoreType.DMA
    whole = pl.BlockSpec(memory_space=pltpu.VMEM)
    far = pl.BlockSpec(memory_space=pl.ANY)
    return pl.pallas_call(
        functools.partial(finish_kernel, n),
        in_specs=[whole] + [far] * 4,
        out_specs=whole,
        out_shape=jax.ShapeDtypeStruct((local, width), jnp.bfloat16),
        scratch_shapes=[
            pltpu.VMEM(y.shape, jnp.bfloat16),
            pltpu.VMEM((n, feats, width), jnp.bfloat16),
            pltpu.VMEM((steps, local, width // steps), jnp.float32),
            pltpu.VMEM((steps, local, width // steps), jnp.bfloat16),
            pltpu.VMEM((steps, local, width // steps), jnp.bfloat16),
            dma((n, 2)), dma((n, 2)), dma((n // 2, 2, 2)), dma((steps,)), dma((steps,)),
        ],
        compiler_params=pltpu.CompilerParams(
            collective_id=1, has_side_effects=True, vmem_limit_bytes=52 << 20
        ),
        cost_estimate=pl.CostEstimate(
            flops=2 * 2 * local * n * feats * width, bytes_accessed=2 * n * feats * width, transcendentals=0
        ),
    )(y, proj_diff, proj_win, other_diff, other_win)


def split_body(
    tokens, norm_gain, query_diff, key_diff, value_diff, lam, output_norm_gain,
    query_win, keyval_win, sink, proj_diff, proj_win,
):
    n = lax.axis_size("sp")
    scal = jnp.stack([jnp.pad(lam, (0, LANES - lam.shape[0])), jnp.pad(sink, (0, LANES - sink.shape[0]))])
    scal = jnp.pad(scal, ((0, 6), (0, 0)))
    res, other_diff, other_win, both = project(
        n, tokens, norm_gain, query_diff, query_win, key_diff, value_diff, keyval_win, proj_diff, proj_win, scal
    )
    y = attend(n, both, res, output_norm_gain)
    return finish(n, y, proj_diff, proj_win, other_diff, other_win)


def splits(mesh, tokens, query_diff, query_win, lam, sink):
    parts, n, tp = (mesh.shape[a] for a in ("grp", "sp", "tp"))
    return (
        parts == 2 and tp == 4 and n % 2 == 0
        and lam.shape[0] == 2 * n and sink.shape[0] == 2 * lam.shape[0]
        and tokens.shape[0] == parts * n * tp * WINDOW
        and query_diff.shape[1] == lam.shape[0] * 2 * HEAD and VDIM == 2 * HEAD
        and query_win.shape[1] == sink.shape[0] * HEAD and HEAD == LANES
    )


def solution(mesh):
    placed = (
        P(("grp", "sp", "tp"), None),
        P(),
        P("sp", "tp"),
        P("sp", "tp"),
        P("sp", "tp"),
        P("tp"),
        P(),
        P("sp", "tp"),
        P(None, "sp", None),
        P("tp"),
        P("tp", None),
        P("tp", None),
    )

    def build(body):
        return jax.shard_map(
            body, mesh=mesh, in_specs=placed, out_specs=P(("grp", "sp", "tp"), None), check_vma=False
        )

    general = build(general_body)

    def step(*args):
        tokens, query_diff, lam, query_win, sink = (args[i] for i in (0, 2, 5, 7, 9))
        if splits(mesh, tokens, query_diff, query_win, lam, sink):
            return build(split_body)(*args)
        return general(*args)

    return step
```

profile of v0, /device:TPU:9, one launch (start us, length us, event | category | flops | bytes accessed | tf_op | source)
XLA Modules:
  0.0 219.3 jit_solution(12051785519444824976)
XLA Ops:
  0.0 0.7 pad_bitcast_fusion
  0.7 0.0 copy-start
  0.7 1.2 copy-done
  1.9 0.0 copy-start.1
  1.9 0.7 copy-done.1
  2.6 153.2 %shard_map.118 = (bf16[2,4,4,128,640]{4,3,2,1,0:T(8,128)(2,1)}, bf16[512,4096]{1,0:T(8,128)(2,1)}, bf16[512,4096]{1,0:T(8,128)(2,1)}, f32[2,8,128]{2,1,0:T(8,128)S(1)}) custom-call(bf16[128,4096]{1,0:T(8,128)(2,1)S(1)} %copy-done, f32[1,4096]{1,0:T(1,128)S(1)} %bitcast.6, bf16[1024,512]{1,0:T(8,128)(2,1)} %qd.1, bf16[1024,512]{1,0:T(8,128)(2,1)} %qw.1, ...), custom_call_target="tpu_custom_call" | custom-call | flops 10737418240 | bytes 22020096 | tf_op jit(solution)/shard_map/pallas_call | solution.py:542
  155.8 0.0 copy-start.2
  155.8 0.6 copy-done.2
  156.4 12.4 %shard_map.119.y_ref = bf16[4,2,128,512]{3,2,1,0:T(8,128)(2,1)} custom-call(f32[2,8,128]{2,1,0:T(8,128)} %copy-done.2, bf16[2,4,4,128,640]{4,3,2,1,0:T(8,128)(2,1)} %get-tuple-element.10.res_ref, f32[1,256]{1,0:T(1,128)} %bitcast.7), custom_call_target="tpu_custom_call" | custom-call | flops 3221225472 | bytes 5242880 | tf_op jit(solution)/shard_map/pallas_call | solution.py:645
  168.9 49.4 %shard_map.120 = bf16[128,4096]{1,0:T(8,128)(2,1)S(1)} custom-call(bf16[4,2,128,512]{3,2,1,0:T(8,128)(2,1)} %shard_map.119.y_ref, bf16[512,4096]{1,0:T(8,128)(2,1)} %pd.3, bf16[512,4096]{1,0:T(8,128)(2,1)} %pw.3, bf16[512,4096]{1,0:T(8,128)(2,1)} %get-tuple-element.11.opd, bf16[512,4096]{1,0:T(8,128)(2,1)} %get-tuple-element.12.opw), custom_call_target="tpu_custom_call" | custom-call | flops 4294967296 | bytes 16777216 | tf_op jit(solution)/shard_map/pallas_call | solution.py:750
  218.3 1.0 copy.14
  (1 shorter events, 0.0 us)
Async XLA Ops:
  0.7 1.2 copy-start
  1.9 0.7 copy-start.1
  155.8 0.6 copy-start.2
where the time goes:
time: 221 us; the launch traced here: 219 us
  Pallas kernels  215 us (97%)
  local copies, waits for them, and re-layouts  4.18 us (2%)
    pallas_call x1, Pallas kernels, project(): pl.pallas_call(functools.partial(project_kernel, n, held), in_specs=[whol...  153 us
    pallas_call x1, Pallas kernels, finish(): pl.pallas_call(functools.partial(finish_kernel, n), in_specs=[whole] + [f...  49.4 us
    pallas_call x1, Pallas kernels, attend(): pl.pallas_call(functools.partial(attend_kernel, n), grid=(n,), in_specs=[...  12.4 us

commit v1 on v0

--- a/solution.py
+++ b/solution.py
@@ -259,10 +259,35 @@
     pl.semaphore_wait(barrier, len(devices))
 
 
+def arrivals(n, here):
+    times = []
+    for k in range(1, n):
+        for h in range(CHUNKS):
+            at = k - 1 + (h + 1) / CHUNKS
+            if here - k >= 0:
+                times.append((at, "z", here - k, h, 0, k))
+            if here + k < n:
+                times.append((at + 0.01, "z", here + k, h, 1, k))
+    times.sort()
+    clock = 0.0
+    beside = []
+    for at, zz, h in [(0.0, here, h) for h in range(CHUNKS)] + [(e[0], e[2], e[3]) for e in times]:
+        clock = max(clock, at) + 1 / CHUNKS
+        beside.append((clock + 0.05, "x", zz, h, 0, 0))
+    return times + beside
+
+
+def order(n, here):
+    def start(zz):
+        return (zz + 1 if zz < here else n - zz, abs(zz - here))
+
+    return sorted((zz for zz in range(n) if zz != here), key=start)
+
+
 def project_kernel(
     n, held, tok_ref, gain_ref, qd, qw, kd, vd, kvw, pd, pw, scal_ref,
     res_ref, opd, opw, oscal_ref,
-    rows_ref, w_ref, zs, zr, xs, xr, cs, cr, ws, wr, ys, yr, own_sem, rs, rr, ps, pr, scal_s, scal_r,
+    rows_ref, w_ref, sum_ref, zs, zr, xs, xr, cs, cr, ws, wr, ys, yr, own_sem, rs, rr, ps, pr, scal_s, scal_r,
 ):
     g, z, t, x, c, t_x, t_c = place()
     local, _ = tok_ref.shape
@@ -272,14 +297,15 @@
     group = WIN_HEADS // KV_HEADS
     mats = (qd, qw, kd, vd, kvw)
     core = (g, z, t_c)
+    f32, bf16 = jnp.float32, jnp.bfloat16
 
     def block(zz, h, tt):
         return rows_ref.at[zz, h, pl.ds(pl.multiple_of(tt * part, part), part)]
 
     for h in range(CHUNKS):
-        v = tok_ref[h * part:(h + 1) * part, :].astype(jnp.float32)
+        v = tok_ref[h * part:(h + 1) * part, :].astype(f32)
         v = v * lax.rsqrt(jnp.mean(v * v, axis=-1, keepdims=True) + EPS) * gain_ref[...]
-        rows_ref[z, h, pl.ds(pl.multiple_of(t * part, part), part), :] = v.astype(jnp.bfloat16)
+        rows_ref[z, h, pl.ds(pl.multiple_of(t * part, part), part), :] = v.astype(bf16)
     oscal_ref[c] = scal_ref[...]
 
     greet(
@@ -287,70 +313,55 @@
         + [(g, z, t_x), (1 - g, z, t)]
     )
 
-    def w_own(zz, yy, m):
-        return w_ref.at[pl.ds(pl.multiple_of(zz * depth + yy * half, half), half), m * LANES:(m + 1) * LANES]
-
-    def w_copy(i, cc, m, remote_half):
-        dz = c * held + i
-        lanes = slice((2 * i + cc) * LANES, (2 * i + cc + 1) * LANES)
+    def w_half(zz, yy, m):
+        at = pl.ds(pl.multiple_of(zz * depth + yy * half, half), half)
+        return w_ref.at[at, m * LANES:(m + 1) * LANES]
+
+    def source(dz, i, cc, m, at):
         if m == MATS - 1:
-            source = kvw.at[(2 * (x * n + dz)) // group]
-            lanes = slice(cc * LANES, (cc + 1) * LANES)
-        else:
-            source = mats[m]
-        if remote_half:
-            return remote(
-                source.at[pl.ds(pl.multiple_of(g * half, half), half), lanes], w_own(z, g, m),
-                ws.at[i, cc, m], wr.at[z, m], (g, dz, 2 * x + cc),
-            )
-        target = w_ref.at[pl.ds(pl.multiple_of(z * depth, depth), depth), m * LANES:(m + 1) * LANES]
-        return source.at[:, lanes], target
-
-    def each_weight(act):
-        for m in range(MATS):
-            for i in range(held):
-                for cc in range(2):
-                    act(m, i, cc)
-
-    def w_start(m, i, cc):
-        dz = c * held + i
-
-        @pl.when(dz != z)
-        def _():
-            w_copy(i, cc, m, True).start()
-
-    def w_start_own(m, i, cc):
-        dz = c * held + i
-        source, target = w_copy(i, cc, m, False)
-
-        @pl.when((dz == z) & (cc == c))
-        def _():
-            pltpu.make_async_copy(source, target, own_sem.at[m]).start()
-
-        @pl.when((dz == z) & (cc != c))
-        def _():
-            remote(source, target, ws.at[i, cc, m], own_sem.at[m], core).start()
-
-    def w_wait_send(m, i, cc):
-        dz = c * held + i
-        source, target = w_copy(i, cc, m, False)
-
-        @pl.when(dz != z)
-        def _():
-            w_copy(i, cc, m, True).wait_send()
-
-        @pl.when((dz == z) & (cc != c))
-        def _():
-            remote(source, target, ws.at[i, cc, m], own_sem.at[m], core).wait_send()
-
-    def z_copy(way, k, h):
-        zz = z - k if way == 0 else z + k
-        to = z + 1 if way == 0 else z - 1
+            return kvw.at[(2 * (x * n + dz)) // group, at, cc * LANES:(cc + 1) * LANES]
+        return mats[m].at[at, (2 * i + cc) * LANES:(2 * i + cc + 1) * LANES]
+
+    def w_copy(here, dz, cc, m):
+        at = pl.ds(pl.multiple_of(g * half, half), half)
+        return remote(
+            source(dz, dz % held, cc, m, at), w_half(here, g, m),
+            ws.at[dz % held, cc, m], wr.at[here, m], (g, dz, 2 * x + cc),
+        )
+
+    def w_each(here, way, act):
+        for cs_ in range(2):
+            @pl.when(c == cs_)
+            def _():
+                for m in range(MATS):
+                    for dz in range(cs_ * held, (cs_ + 1) * held):
+                        if (dz > here) if way == 0 else (dz < here):
+                            for cc in range(2):
+                                act(w_copy(here, dz, cc, m))
+
+    def own_copy(here, cc, m):
+        at = pl.ds(0, depth)
+        target = w_ref.at[here * depth:(here + 1) * depth, m * LANES:(m + 1) * LANES]
+        return source(here, here % held, cc, m, at), target
+
+    def own_each(here, near, away):
+        for cc in range(2):
+            for m in range(MATS):
+                a, b = own_copy(here, cc, m)
+
+                if near is not None:
+                    @pl.when((c == here // held) & (c == cc))
+                    def _():
+                        near(pltpu.make_async_copy(a, b, own_sem.at[m]))
+
+                @pl.when((c == here // held) & (c != cc))
+                def _():
+                    away(remote(a, b, ws.at[here % held, cc, m], own_sem.at[m], core))
+
+    def z_copy(zz, h, way, here):
+        k = abs(zz - here)
+        to = here + 1 if way == 0 else here - 1
         return remote(block(zz, h, t), block(zz, h, t), zs.at[way, k, h], zr.at[way, k + 1, h], (g, to, t))
-
-    def z_wait(way, k, h):
-        zz = z - k if way == 0 else z + k
-        remote(block(zz, h, t), block(zz, h, t), zs.at[way, k, h], zr.at[way, k, h], core).wait_recv()
 
     def x_copy(zz, h):
         return remote(block(zz, h, t), block(zz, h, t), xs.at[zz, h], xr.at[zz, h], (g, z, t_x))
@@ -360,175 +371,168 @@
         return remote(block(zz, h, tt), block(zz, h, tt), cs.at[zz, xx, h], cr.at[zz, xx, h], core)
 
     def y_copy(zz, m):
-        return remote(w_own(zz, g, m), w_own(zz, g, m), ys.at[zz, m], yr.at[zz, m], (1 - g, z, t))
-
-    each_weight(w_start)
-    for h in range(CHUNKS):
-        @pl.when(z < n - 1)
-        def _(h=h):
-            z_copy(0, 0, h).start()
-
-        @pl.when(z > 0)
-        def _(h=h):
-            z_copy(1, 0, h).start()
-
-        x_copy(z, h).start()
-        c_copy(z, x, h).start()
+        return remote(w_half(zz, g, m), w_half(zz, g, m), ys.at[zz, m], yr.at[zz, m], (1 - g, z, t))
+
+    def forward(zz, m):
+        remote(w_half(zz, g, m), w_half(zz, g, m), ys.at[zz, m], wr.at[zz, m], core).wait_recv()
+        y_copy(zz, m).start()
+
+    def crossed(zz):
+        for m in range(MATS):
+            remote(w_half(zz, 1 - g, m), w_half(zz, 1 - g, m), ys.at[zz, m], yr.at[zz, m], core).wait_recv()
+
     scal_copy = remote(scal_ref, oscal_ref.at[c], scal_s, scal_r, core)
-    scal_copy.start()
-    each_weight(w_start_own)
+
+    def gather(here):
+        for h in range(CHUNKS):
+            if here < n - 1:
+                z_copy(here, h, 0, here).start()
+            if here > 0:
+                z_copy(here, h, 1, here).start()
+            x_copy(here, h).start()
+            c_copy(here, x, h).start()
+        scal_copy.start()
+        own_each(here, lambda copy: copy.start(), lambda copy: copy.start())
+        if here == 0:
+            w_each(here, 0, lambda copy: copy.start())
+        if here == n - 1:
+            w_each(here, 1, lambda copy: copy.start())
+        first = order(n, here)[0]
+        begin = first + 1 if first < here else n - first
+        events = arrivals(n, here)
+        events += [(begin + 0.5 * (m + 1), "w", first, m, 0, 0) for m in range(MATS)]
+        for at, kind, zz, h, way, k in sorted(events):
+            if kind == "z":
+                remote(block(zz, h, t), block(zz, h, t), zs.at[way, k, h], zr.at[way, k, h], core).wait_recv()
+                if (here < n - 1) if way == 0 else (here > 0):
+                    z_copy(zz, h, way, here).start()
+                x_copy(zz, h).start()
+                c_copy(zz, x, h).start()
+                if h == CHUNKS - 1 and zz == (0 if way == 0 else n - 1):
+                    w_each(here, way, lambda copy: copy.start())
+            elif kind == "x":
+                x_copy(zz, h).wait_recv()
+                c_copy(zz, 1 - x, h).start()
+            else:
+                forward(zz, h)
+
+    for here in range(n):
+        pl.when(z == here)(functools.partial(gather, here))
+
     proj_copies = [remote(pd, opd, ps.at[0], pr.at[0], core), remote(pw, opw, ps.at[1], pr.at[1], core)]
     for copy in proj_copies:
         copy.start()
 
-    def sides(k, act):
-        @pl.when(z - k >= 0)
-        def _():
-            act(z - k, 0)
-
-        @pl.when((z + k < n) & (k > 0))
-        def _():
-            act(z + k, 1)
-
-    for d in range(1, n):
-        def forward(zz, way):
-            def one(m):
-                remote(w_own(zz, g, m), w_own(zz, g, m), ys.at[zz, m], wr.at[zz, m], core).wait_recv()
-                y_copy(zz, m).start()
-
-            for m in range(MATS):
-                one(m)
-
-        sides(d, forward)
-
-    def stage_a(e):
-        k, h = e // CHUNKS, e % CHUNKS
-
-        def act(zz, way):
-            z_wait(way, k, h)
-
-            @pl.when(z < n - 1 if way == 0 else z > 0)
-            def _():
-                z_copy(way, k, h).start()
-
-            x_copy(zz, h).start()
-            c_copy(zz, x, h).start()
-
-        sides(k, act)
-
-    def stage_b(e):
-        k, h = e // CHUNKS, e % CHUNKS
-
-        def act(zz, way):
-            x_copy(zz, h).wait_recv()
-            c_copy(zz, 1 - x, h).start()
-
-        sides(k, act)
-
-    def stage_c(e, carry):
-        k, h = e // CHUNKS, e % CHUNKS
-
-        def act(zz, way):
-            for xx in range(2):
+    sources = []
+    for j in range(n - 1):
+        zz = order(n, 0)[j] + 0 * z
+        for here in range(1, n):
+            zz = jnp.where(z == here, order(n, here)[j], zz)
+        sources.append(zz)
+
+    quad = rows_ref.shape[2]
+
+    def partial_sum(zz, at, size):
+        k = pl.ds(pl.multiple_of(at, half), size)
+        left = rows_ref[zz, :, :, k].reshape(CHUNKS * quad, size)
+        return jnp.dot(left, w_ref[k, :], preferred_element_type=f32)
+
+    def opening(zz, carry):
+        for xx in range(2):
+            for h in range(CHUNKS):
                 c_copy(zz, xx, h).wait_recv()
-            res_ref[c, zz, h] = jnp.dot(
-                rows_ref[zz, h], w_ref[...], preferred_element_type=jnp.float32
-            ).astype(jnp.bfloat16)
-
-        sides(k, act)
+        sum_ref[zz] = partial_sum(zz, z * depth, depth)
         return carry
 
-    def r_copies(zz, h):
+    def add(at):
+        def one(zz, carry):
+            sum_ref[zz] += partial_sum(zz, at, half)
+            return carry
+
+        lax.fori_loop(0, n, one, 0)
+
+    def r_copies(zz):
         copies = [remote(
-            res_ref.at[c, zz, h, :, 2 * LANES:], res_ref.at[c, zz, h, :, 2 * LANES:],
-            rs.at[zz, h, 0], rr.at[zz, h, 0], core,
+            res_ref.at[c, zz, :, :, 2 * LANES:], res_ref.at[c, zz, :, :, 2 * LANES:],
+            rs.at[zz, 0], rr.at[zz, 0], core,
         )]
         for xx in range(2):
             at = pl.ds(pl.multiple_of((2 * xx + 1 - c) * part, part), part)
             copies.append(remote(
-                res_ref.at[c, zz, h, at, :2 * LANES], res_ref.at[c, zz, h, at, :2 * LANES],
-                rs.at[zz, h, 1 + xx], rr.at[zz, h, 1 + xx], core,
+                res_ref.at[c, zz, :, at, :2 * LANES], res_ref.at[c, zz, :, at, :2 * LANES],
+                rs.at[zz, 1 + xx], rr.at[zz, 1 + xx], core,
             ))
         return copies
 
-    def stage_d(e, carry):
-        k, h = e // CHUNKS, e % CHUNKS
-
-        def act(zz, way):
-            for copy in r_copies(zz, h):
+    for m in range(MATS):
+        a, b = own_copy(0, 0, m)
+        pltpu.make_async_copy(a, b, own_sem.at[m]).wait()
+    late = sources[1:]
+
+    def forwards(lo, hi):
+        for m in range(lo, hi):
+            for zz in late:
+                forward(zz, m)
+
+    forwards(0, 1)
+    lax.fori_loop(0, n, opening, 0)
+    forwards(1, 2)
+    add(sources[0] * depth + g * half)
+    crossed(sources[0])
+    add(sources[0] * depth + (1 - g) * half)
+    forwards(2, MATS)
+    for zz in late:
+        add(zz * depth + g * half)
+    for zz in late[:-1]:
+        crossed(zz)
+        add(zz * depth + (1 - g) * half)
+    crossed(sources[-1])
+
+    def closing(zz, carry):
+        total = sum_ref[zz] + partial_sum(zz, sources[-1] * depth + (1 - g) * half, half)
+
+        @pl.when(zz > 0)
+        def _():
+            for copy in r_copies(zz - 1):
                 copy.start()
 
-        sides(k, act)
+        res_ref[c, zz] = total.astype(bf16).reshape(CHUNKS, quad, MATS * LANES)
         return carry
 
-    for e in range(CHUNKS - 1):
-        stage_b(e)
-
-    last = n * CHUNKS
-
-    def upto(e):
-        return jnp.maximum(jnp.minimum(2 * (e - 2 * CHUNKS + 1), e - 1), 0)
-
-    def weights_ready():
-        for m in range(MATS):
-            source, target = w_copy(0, 0, m, False)
-            pltpu.make_async_copy(source, target, own_sem.at[m]).wait()
-        for d in range(1, n):
-            def arrived(zz, way):
-                for m in range(MATS):
-                    remote(w_own(zz, 1 - g, m), w_own(zz, 1 - g, m), ys.at[zz, m], yr.at[zz, m], core).wait_recv()
-
-            sides(d, arrived)
-
-    def step(e, carry):
-        @pl.when(e < last)
-        def _():
-            stage_a(e)
-
-        @pl.when(e < last + 1)
-        def _():
-            stage_b(e - 1)
-
-        pl.when(e == 2 * CHUNKS)(weights_ready)
-        lax.fori_loop(upto(e - 2), upto(e - 1), stage_d, 0)
-        lax.fori_loop(upto(e - 1), upto(e), stage_c, 0)
-        return carry
-
-    lax.fori_loop(CHUNKS, last + 2, step, 0)
+    lax.fori_loop(0, n, closing, 0)
     for copy in proj_copies + [scal_copy]:
         copy.wait()
-    each_weight(w_wait_send)
-    lax.fori_loop(upto(last), upto(last + 1), stage_d, 0)
-
-    def drain(e, carry):
-        k, h = e // CHUNKS, e % CHUNKS
-
-        def act(zz, way):
-            @pl.when(z < n - 1 if way == 0 else z > 0)
-            def _():
-                z_copy(way, k, h).wait_send()
-
+    for copy in r_copies(n - 1):
+        copy.start()
+
+    def drain(here):
+        for way in range(2):
+            if (here < n - 1) if way == 0 else (here > 0):
+                w_each(here, way, lambda copy: copy.wait_send())
+                for zz in (range(here + 1) if way == 0 else range(here, n)):
+                    for h in range(CHUNKS):
+                        z_copy(zz, h, way, here).wait_send()
+        own_each(here, None, lambda copy: copy.wait_send())
+
+    for here in range(n):
+        pl.when(z == here)(functools.partial(drain, here))
+
+    def finished(zz, carry):
+        for h in range(CHUNKS):
             x_copy(zz, h).wait_send()
             for xx in range(2):
                 c_copy(zz, xx, h).wait_send()
-            for copy in r_copies(zz, h):
-                copy.wait()
-
-        sides(k, act)
-
-        @pl.when((k == 0) & (z > 0))
+
+        @pl.when(zz != z)
         def _():
-            z_copy(1, 0, h).wait_send()
-
-        return carry
-
-    lax.fori_loop(0, last, drain, 0)
-    for d in range(1, n):
-        def sent(zz, way):
             for m in range(MATS):
                 y_copy(zz, m).wait_send()
 
-        sides(d, sent)
+        for copy in r_copies(zz):
+            copy.wait()
+        return carry
+
+    lax.fori_loop(0, n, finished, 0)
 
 
 def project(n, tokens, norm_gain, query_diff, query_win, key_diff, value_diff, keyval_win, proj_diff, proj_win, scal):
@@ -552,12 +556,13 @@
         scratch_shapes=[
             pltpu.VMEM((n, CHUNKS, 4 * local // CHUNKS, width), jnp.bfloat16),
             pltpu.VMEM((width, cols), jnp.bfloat16),
+            pltpu.VMEM((n, 4 * local, cols), jnp.float32),
             dma((2, n, CHUNKS)), dma((2, n + 1, CHUNKS)),
             dma((n, CHUNKS)), dma((n, CHUNKS)),
             dma((n, 2, CHUNKS)), dma((n, 2, CHUNKS)),
             dma((held, 2, MATS)), dma((n, MATS)),
             dma((n, MATS)), dma((n, MATS)), dma((MATS,)),
-            dma((n, CHUNKS, 3)), dma((n, CHUNKS, 3)),
+            dma((n, 3)), dma((n, 3)),
             dma((2,)), dma((2,)), dma, dma,
         ],
         compiler_params=pltpu.CompilerParams(

time: 221 us -> 206 us (0.932)
  Pallas kernels: 215 us -> 199 us
    pallas_call x1, Pallas kernels: 153 us -> 137 us  [project(): pl.pallas_call(functools.partial(project_kernel, n, held), in_specs=[whol...]
where the time goes in v1:
time: 206 us; the launch traced here: 204 us
  Pallas kernels  199 us (97%)
  local copies, waits for them, and re-layouts  4.18 us (2%)
    pallas_call x1, Pallas kernels, project(): pl.pallas_call(functools.partial(project_kernel, n, held), in_specs=[whol...  137 us
    pallas_call x1, Pallas kernels, finish(): pl.pallas_call(functools.partial(finish_kernel, n), in_specs=[whole] + [f...  50.3 us
    pallas_call x1, Pallas kernels, attend(): pl.pallas_call(functools.partial(attend_kernel, n), grid=(n,), in_specs=[...  12.5 us

profile of v1, /device:TPU:9, one launch (start us, length us, event | category | flops | bytes accessed | tf_op | source)
XLA Modules:
  0.0 203.6 jit_solution(1171105078157914498)
XLA Ops:
  0.0 0.7 pad_bitcast_fusion
  0.7 0.0 copy-start
  0.7 1.2 copy-done
  1.9 0.0 copy-start.1
  1.9 0.7 copy-done.1
  2.6 136.6 %shard_map.118 = (bf16[2,4,4,128,640]{4,3,2,1,0:T(8,128)(2,1)}, bf16[512,4096]{1,0:T(8,128)(2,1)}, bf16[512,4096]{1,0:T(8,128)(2,1)}, f32[2,8,128]{2,1,0:T(8,128)S(1)}) custom-call(bf16[128,4096]{1,0:T(8,128)(2,1)S(1)} %copy-done, f32[1,4096]{1,0:T(1,128)S(1)} %bitcast.6, bf16[1024,512]{1,0:T(8,128)(2,1)} %qd.1, bf16[1024,512]{1,0:T(8,128)(2,1)} %qw.1, ...), custom_call_target="tpu_custom_call" | custom-call | flops 10737418240 | bytes 22020096 | tf_op jit(solution)/shard_map/pallas_call | solution.py:546
  139.2 0.0 copy-start.2
  139.2 0.6 copy-done.2
  139.8 12.5 %shard_map.119.y_ref = bf16[4,2,128,512]{3,2,1,0:T(8,128)(2,1)} custom-call(f32[2,8,128]{2,1,0:T(8,128)} %copy-done.2, bf16[2,4,4,128,640]{4,3,2,1,0:T(8,128)(2,1)} %get-tuple-element.10.res_ref, f32[1,256]{1,0:T(1,128)} %bitcast.7), custom_call_target="tpu_custom_call" | custom-call | flops 3221225472 | bytes 5242880 | tf_op jit(solution)/shard_map/pallas_call | solution.py:650
  152.3 50.3 %shard_map.120 = bf16[128,4096]{1,0:T(8,128)(2,1)S(1)} custom-call(bf16[4,2,128,512]{3,2,1,0:T(8,128)(2,1)} %shard_map.119.y_ref, bf16[512,4096]{1,0:T(8,128)(2,1)} %pd.3, bf16[512,4096]{1,0:T(8,128)(2,1)} %pw.3, bf16[512,4096]{1,0:T(8,128)(2,1)} %get-tuple-element.11.opd, bf16[512,4096]{1,0:T(8,128)(2,1)} %get-tuple-element.12.opw), custom_call_target="tpu_custom_call" | custom-call | flops 4294967296 | bytes 16777216 | tf_op jit(solution)/shard_map/pallas_call | solution.py:755
  202.6 1.0 copy.14
  (1 shorter events, 0.0 us)
Async XLA Ops:
  0.7 1.2 copy-start
  1.9 0.7 copy-start.1
  139.2 0.6 copy-start.2

commit v2 on v1

--- a/solution.py
+++ b/solution.py
@@ -284,13 +284,14 @@
     return sorted((zz for zz in range(n) if zz != here), key=start)
 
 
-def project_kernel(
-    n, held, tok_ref, gain_ref, qd, qw, kd, vd, kvw, pd, pw, scal_ref,
-    res_ref, opd, opw, oscal_ref,
-    rows_ref, w_ref, sum_ref, zs, zr, xs, xr, cs, cr, ws, wr, ys, yr, own_sem, rs, rr, ps, pr, scal_s, scal_r,
+def whole_kernel(
+    n, held, tok_ref, gain_ref, qd, qw, kd, vd, kvw, pd, pw, scal_ref, out_gain_ref,
+    out_ref,
+    rows_ref, w_ref, sum_ref, res_ref, oscal_ref, p_ref, v_ref, y_ref, got_ref, mine_ref, away_ref, theirs_ref,
+    zs, zr, xs, xr, cs, cr, ws, wr, ys, yr, own_sem, rs, rr, ps, pr, load, scal_s, scal_r, hs, hr, ds, dr,
 ):
     g, z, t, x, c, t_x, t_c = place()
-    local, _ = tok_ref.shape
+    local, width = tok_ref.shape
     part = local // CHUNKS
     depth = qd.shape[0]
     half = depth // 2
@@ -419,8 +420,14 @@
     for here in range(n):
         pl.when(z == here)(functools.partial(gather, here))
 
-    proj_copies = [remote(pd, opd, ps.at[0], pr.at[0], core), remote(pw, opw, ps.at[1], pr.at[1], core)]
-    for copy in proj_copies:
+    proj_copies, loads = [], []
+    for i in range(held):
+        for j, ref in enumerate((pd, pw)):
+            rows = ref.at[i * VDIM:(i + 1) * VDIM]
+            at = p_ref.at[c * held + i, j * VDIM:(j + 1) * VDIM]
+            loads.append(pltpu.make_async_copy(rows, at, load.at[i, j]))
+            proj_copies.append(remote(rows, at, ps.at[i, j], pr.at[i, j], core))
+    for copy in loads + proj_copies:
         copy.start()
 
     sources = []
@@ -500,10 +507,165 @@
         return carry
 
     lax.fori_loop(0, n, closing, 0)
-    for copy in proj_copies + [scal_copy]:
-        copy.wait()
+    scal_copy.wait()
     for copy in r_copies(n - 1):
         copy.start()
+
+    def exchanged(zz, carry):
+        for copy in r_copies(zz):
+            copy.wait_recv()
+        return carry
+
+    lax.fori_loop(0, n, exchanged, 0)
+
+    rows = n * 4 * local
+    factor = HEAD ** (-0.5) * math.log2(math.e)
+    for i in range(2):
+        v_ref[:, i * LANES:(i + 1) * LANES] = res_ref[i, :, :, :, 3 * LANES:4 * LANES].reshape(rows, LANES)
+
+    level = oscal_ref[z // held]
+    level_row = lax.broadcasted_iota(jnp.int32, level.shape, 0)
+    level_lane = lax.broadcasted_iota(jnp.int32, level.shape, 1)
+
+    def scalar(row, lane):
+        picked = jnp.where((level_row == row) & (level_lane == lane), level, 0.0)
+        return jnp.sum(jnp.sum(picked, axis=1, keepdims=True), axis=0, keepdims=True)
+
+    lam = scalar(0, z % held)
+    sinks = [scalar(1, 2 * (z % held) + i) for i in range(2)]
+    first = lax.broadcasted_iota(jnp.int32, (2 * local, 1), 0) < local
+    sink = jnp.where(first, sinks[0], sinks[1])
+
+    distant = []
+    for j in range(n):
+        zz = 0 * z
+        for here in range(n):
+            far = sorted(range(n), key=lambda o: -abs(o - here))[j]
+            zz = jnp.where(z == here, far, zz)
+        distant.append(zz)
+
+    def pick(values, j):
+        value = values[0]
+        for i in range(1, len(values)):
+            value = jnp.where(j == i, values[i], value)
+        return value
+
+    def piece(i, zz, tt, m):
+        at = pl.ds(pl.multiple_of(tt * part, part), part)
+        return res_ref[i, zz, :, at, m * LANES:(m + 1) * LANES].reshape(local, LANES)
+
+    def y_copy_to(zz, xx):
+        return remote(y_ref.at[zz, xx], got_ref.at[z, xx], hs.at[zz, xx], hr.at[z, xx], (g, zz, t))
+
+    def y_wait(zz, xx):
+        return remote(got_ref.at[zz, xx], got_ref.at[zz, xx], hs.at[zz, xx], hr.at[zz, xx], (g, z, t_x))
+
+    def windowed(zz, tt, xx):
+        b = 4 * zz + tt
+
+        def banded(i):
+            pieces = []
+            for o in (-1, 0, 1):
+                o = jnp.clip(b + o, 0, 4 * n - 1)
+                pieces.append(piece(i, o // 4, o % 4, 4))
+            return jnp.concatenate(pieces, axis=0)
+
+        q = jnp.concatenate([piece(i, zz, tt, 1) for i in range(2)], axis=0)
+        scores = lax.dot_general(
+            q, banded(0), (((1,), (1,)), ((), ())), preferred_element_type=f32
+        ) * HEAD ** (-0.5)
+        r_index = lax.broadcasted_iota(jnp.int32, scores.shape, 0) % local
+        k_index = lax.broadcasted_iota(jnp.int32, scores.shape, 1)
+        spot = (b - 1) * local + k_index
+        valid = (jnp.abs(k_index - local - r_index) <= WINDOW) & (spot >= 0) & (spot < rows)
+        scores = jnp.where(valid, scores, -jnp.inf)
+        top = jnp.maximum(jnp.max(scores, axis=-1, keepdims=True), sink)
+        expo = jnp.exp(scores - top)
+        weights = expo / (jnp.sum(expo, axis=-1, keepdims=True) + jnp.exp(sink - top))
+        out = jnp.dot(weights.astype(bf16), banded(1), preferred_element_type=f32).astype(bf16)
+        for i in range(2):
+            y_ref[zz, xx, :, VDIM + i * LANES:VDIM + (i + 1) * LANES] = out[i * local:(i + 1) * local]
+
+    def attend(step, carry):
+        pairs = n // 2
+        xx = jnp.where(step < pairs, 1 - x, x)
+        tt = 2 * xx + c
+        j = step % pairs
+        zzs = [pick(distant[i::2], j) for i in range(2)]
+        maps = []
+        for m in range(2):
+            q = jnp.concatenate([piece(m, zz, tt, 0) for zz in zzs], axis=0)
+            keys = res_ref[m, :, :, :, 2 * LANES:3 * LANES].reshape(rows, LANES)
+            scores = lax.dot_general(q, keys, (((1,), (1,)), ((), ())), preferred_element_type=f32)
+            top = jnp.max(scores, axis=-1, keepdims=True)
+            expo = jnp.exp2((scores - top) * factor)
+            total = jnp.sum(expo, axis=-1, keepdims=True)
+            out = jnp.dot(expo.astype(bf16), v_ref[...], preferred_element_type=f32)
+            maps.append(out / total)
+        d = maps[0] - lam * maps[1]
+        d = d * lax.rsqrt(jnp.mean(d * d, axis=-1, keepdims=True) + EPS) * out_gain_ref[...]
+        d = d.astype(bf16)
+        for i, zz in enumerate(zzs):
+            y_ref[zz, xx, :, :VDIM] = d[i * local:(i + 1) * local]
+        for zz in zzs:
+            windowed(zz, tt, xx)
+        for zz in zzs:
+            @pl.when(zz != z)
+            def _():
+                y_copy_to(zz, xx).start()
+        return carry
+
+    lax.fori_loop(0, n, attend, 0)
+    got_ref[z] = y_ref[z]
+    for copy in loads + proj_copies:
+        copy.wait()
+
+    steps = mine_ref.shape[0]
+    wide = width // steps
+
+    def others(act):
+        for d in range(n - 1, 0, -1):
+            pl.when(z - d >= 0)(functools.partial(act, z - d))
+            pl.when(z + d < n)(functools.partial(act, z + d))
+
+    def product(j, xx):
+        total = jnp.zeros((local, wide), f32)
+        at = pl.ds(pl.multiple_of(j * wide, wide), wide)
+        for zz in range(n):
+            total = total + jnp.dot(got_ref[zz, xx], p_ref[zz, :, at], preferred_element_type=f32)
+        return total
+
+    def d_copy(j):
+        return remote(away_ref.at[j], theirs_ref.at[j], ds.at[j], dr.at[j], (g, z, t_x))
+
+    others(lambda zz: y_wait(zz, 1 - x).wait_recv())
+
+    def send(j, carry):
+        value = product(j, 1 - x).astype(bf16)
+
+        @pl.when(j > 0)
+        def _():
+            d_copy(j - 1).start()
+
+        away_ref[j] = value
+        return carry
+
+    lax.fori_loop(0, steps, send, 0)
+    others(lambda zz: y_wait(zz, x).wait_recv())
+    d_copy(steps - 1).start()
+
+    def keep(j, carry):
+        mine_ref[j] = product(j, x)
+        return carry
+
+    lax.fori_loop(0, steps, keep, 0)
+    for j in range(steps):
+        d_copy(j).wait_recv()
+        out_ref[:, j * wide:(j + 1) * wide] = (mine_ref[j] + theirs_ref[j].astype(f32)).astype(bf16)
+    for j in range(steps):
+        d_copy(j).wait_send()
+    for xx in (1 - x, x):
+        others(lambda zz: y_copy_to(zz, xx).wait_send())
 
     def drain(here):
         for way in range(2):
@@ -529,249 +691,64 @@
                 y_copy(zz, m).wait_send()
 
         for copy in r_copies(zz):
-            copy.wait()
+            copy.wait_send()
         return carry
 
     lax.fori_loop(0, n, finished, 0)
 
 
-def project(n, tokens, norm_gain, query_diff, query_win, key_diff, value_diff, keyval_win, proj_diff, proj_win, scal):
+def whole(
+    n, tokens, norm_gain, query_diff, query_win, key_diff, value_diff, keyval_win, proj_diff, proj_win, scal,
+    output_norm_gain,
+):
     local, width = tokens.shape
     held = n // 2
     dma = pltpu.SemaphoreType.DMA
-    whole = pl.BlockSpec(memory_space=pltpu.VMEM)
+    inside = pl.BlockSpec(memory_space=pltpu.VMEM)
     far = pl.BlockSpec(memory_space=pl.ANY)
     cols = MATS * LANES
     tok = 4 * local * n
+    feats = VDIM + 2 * HEAD
+    steps = 8
+    quad = 4 * local // CHUNKS
+    bf16, f32 = jnp.bfloat16, jnp.float32
     return pl.pallas_call(
-        functools.partial(project_kernel, n, held),
-        in_specs=[whole, whole] + [far] * 7 + [whole],
-        out_specs=[whole, far, far, whole],
-        out_shape=[
-            jax.ShapeDtypeStruct((2, n, CHUNKS, 4 * local // CHUNKS, cols), jnp.bfloat16),
-            jax.ShapeDtypeStruct(proj_diff.shape, proj_diff.dtype),
-            jax.ShapeDtypeStruct(proj_win.shape, proj_win.dtype),
-            jax.ShapeDtypeStruct((2,) + scal.shape, scal.dtype),
-        ],
+        functools.partial(whole_kernel, n, held),
+        in_specs=[inside, inside] + [far] * 7 + [inside, inside],
+        out_specs=inside,
+        out_shape=jax.ShapeDtypeStruct((local, width), bf16),
         scratch_shapes=[
-            pltpu.VMEM((n, CHUNKS, 4 * local // CHUNKS, width), jnp.bfloat16),
-            pltpu.VMEM((width, cols), jnp.bfloat16),
-            pltpu.VMEM((n, 4 * local, cols), jnp.float32),
+            pltpu.VMEM((n, CHUNKS, quad, width), bf16),
+            pltpu.VMEM((width, cols), bf16),
+            pltpu.VMEM((n, 4 * local, cols), f32),
+            pltpu.VMEM((2, n, CHUNKS, quad, cols), bf16),
+            pltpu.VMEM((2,) + scal.shape, f32),
+            pltpu.VMEM((n, feats, width), bf16),
+            pltpu.VMEM((tok, VDIM), bf16),
+            pltpu.VMEM((n, 2, local, feats), bf16),
+            pltpu.VMEM((n, 2, local, feats), bf16),
+            pltpu.VMEM((steps, local, width // steps), f32),
+            pltpu.VMEM((steps, local, width // steps), bf16),
+            pltpu.VMEM((steps, local, width // steps), bf16),
             dma((2, n, CHUNKS)), dma((2, n + 1, CHUNKS)),
             dma((n, CHUNKS)), dma((n, CHUNKS)),
             dma((n, 2, CHUNKS)), dma((n, 2, CHUNKS)),
             dma((held, 2, MATS)), dma((n, MATS)),
             dma((n, MATS)), dma((n, MATS)), dma((MATS,)),
             dma((n, 3)), dma((n, 3)),
-            dma((2,)), dma((2,)), dma, dma,
+            dma((held, 2)), dma((held, 2)), dma((held, 2)), dma, dma,
+            dma((n, 2)), dma((n, 2)), dma((steps,)), dma((steps,)),
         ],
         compiler_params=pltpu.CompilerParams(
-            collective_id=0, has_side_effects=True, vmem_limit_bytes=52 << 20
+            collective_id=0, has_side_effects=True, vmem_limit_bytes=67043328
         ),
         cost_estimate=pl.CostEstimate(
             flops=2 * tok * width * cols, bytes_accessed=2 * width * (tok + cols), transcendentals=0
         ),
-    )(tokens, norm_gain.reshape(1, width), query_diff, query_win, key_diff, value_diff, keyval_win, proj_diff, proj_win, scal)
-
-
-def attend_kernel(n, scal_ref, res_ref, gain_ref, y_ref, v_ref):
-    z, t = lax.axis_index("sp"), lax.axis_index("tp")
-    c = t % 2
-    zz = pl.program_id(0)
-    chunks, quad, _ = res_ref.shape[2:]
-    part = quad // 4
-    local = part * chunks
-    rows = n * chunks * quad
-    factor = HEAD ** (-0.5) * math.log2(math.e)
-    f32, bf16 = jnp.float32, jnp.bfloat16
-
-    @pl.when(zz == 0)
-    def _():
-        for i in range(2):
-            v_ref[:, i * LANES:(i + 1) * LANES] = res_ref[i, :, :, :, 3 * LANES:4 * LANES].reshape(rows, LANES)
-
-    def own(i, xx, m):
-        at = pl.ds(pl.multiple_of((2 * xx + c) * part, part), part)
-        return res_ref[i, zz, :, at, m * LANES:(m + 1) * LANES].reshape(local, LANES)
-
-    maps = []
-    for m in range(2):
-        q = jnp.concatenate([own(m, xx, 0) for xx in range(2)], axis=0)
-        keys = res_ref[m, :, :, :, 2 * LANES:3 * LANES].reshape(rows, LANES)
-        scores = lax.dot_general(q, keys, (((1,), (1,)), ((), ())), preferred_element_type=f32)
-        top = jnp.max(scores, axis=-1, keepdims=True)
-        expo = jnp.exp2((scores - top) * factor)
-        total = jnp.sum(expo, axis=-1, keepdims=True)
-        out = jnp.dot(expo.astype(bf16), v_ref[...], preferred_element_type=f32)
-        maps.append(out / total)
-    lam = scal_ref[z // (n // 2), 0, z % (n // 2)]
-    d = maps[0] - lam * maps[1]
-    d = d * lax.rsqrt(jnp.mean(d * d, axis=-1, keepdims=True) + EPS) * gain_ref[...]
-    y_ref[0, :, :, :VDIM] = d.astype(bf16).reshape(2, local, VDIM)
-
-    held = n // 2
-    r_index = lax.broadcasted_iota(jnp.int32, (2 * local, 3 * local), 0) % local
-    k_index = lax.broadcasted_iota(jnp.int32, (2 * local, 3 * local), 1)
-    near = jnp.abs(k_index - local - r_index) <= WINDOW
-    first = lax.broadcasted_iota(jnp.int32, (2 * local, 1), 0) < local
-    sinks = [scal_ref[z // held, 1, 2 * (z % held) + i] for i in range(2)]
-    sink = jnp.where(first, sinks[0], sinks[1])
-    for xx in range(2):
-        b = 4 * zz + 2 * xx + c
-
-        def banded(i):
-            pieces = []
-            for s in (-1, 0, 1):
-                o = jnp.clip(b + s, 0, 4 * n - 1)
-                at = pl.ds(pl.multiple_of(o % 4 * part, part), part)
-                pieces.append(res_ref[i, o // 4, :, at, 4 * LANES:5 * LANES].reshape(local, LANES))
-            return jnp.concatenate(pieces, axis=0)
-
-        q = jnp.concatenate([own(i, xx, 1) for i in range(2)], axis=0)
-        scores = lax.dot_general(
-            q, banded(0), (((1,), (1,)), ((), ())), preferred_element_type=f32
-        ) * HEAD ** (-0.5)
-        spot = (b - 1) * local + k_index
-        valid = near & (spot >= 0) & (spot < rows)
-        scores = jnp.where(valid, scores, -jnp.inf)
-        top = jnp.maximum(jnp.max(scores, axis=-1, keepdims=True), sink)
-        expo = jnp.exp(scores - top)
-        weights = expo / (jnp.sum(expo, axis=-1, keepdims=True) + jnp.exp(sink - top))
-        out = jnp.dot(weights.astype(bf16), banded(1), preferred_element_type=f32).astype(bf16)
-        for i in range(2):
-            y_ref[0, xx, :, VDIM + i * LANES:VDIM + (i + 1) * LANES] = out[i * local:(i + 1) * local]
-
-
-def attend(n, scal, res, gain):
-    chunks, quad, _ = res.shape[2:]
-    local = quad * chunks // 4
-    rows = n * chunks * quad
-    feats = VDIM + 2 * HEAD
-    return pl.pallas_call(
-        functools.partial(attend_kernel, n),
-        grid=(n,),
-        in_specs=[
-            pl.BlockSpec(memory_space=pltpu.SMEM),
-            pl.BlockSpec(memory_space=pltpu.VMEM),
-            pl.BlockSpec(memory_space=pltpu.VMEM),
-        ],
-        out_specs=pl.BlockSpec((1, 2, local, feats), lambda i: (i, 0, 0, 0)),
-        out_shape=jax.ShapeDtypeStruct((n, 2, local, feats), jnp.bfloat16),
-        scratch_shapes=[pltpu.VMEM((rows, VDIM), jnp.bfloat16)],
-        cost_estimate=pl.CostEstimate(
-            flops=rows * rows * 2 * (HEAD + VDIM), bytes_accessed=2 * res.size, transcendentals=rows * rows
-        ),
-    )(scal, res, gain.reshape(1, VDIM))
-
-
-def finish_kernel(
-    n, y_ref, pd, pw, opd, opw, out_ref,
-    got_ref, p_ref, mine_ref, away_ref, theirs_ref, ys, yr, load, ds, dr,
-):
-    g, z, t, x, c, t_x, _ = place()
-    held = n // 2
-    local, width = out_ref.shape
-    steps = mine_ref.shape[0]
-    wide = width // steps
-    f32, bf16 = jnp.float32, jnp.bfloat16
-
-    loads = []
-    for i in range(held):
-        for far, at, a, b in ((0, c, pd, pw), (1, 1 - c, opd, opw)):
-            for j, ref in enumerate((a, b)):
-                loads.append(pltpu.make_async_copy(
-                    ref.at[i * VDIM:(i + 1) * VDIM], p_ref.at[at * held + i, j * VDIM:(j + 1) * VDIM],
-                    load.at[i, far, j],
-                ))
-    for copy in loads:
-        copy.start()
-
-    greet([(g, lax.rem(z + i, n), t) for i in range(1, n)] + [(g, z, t_x)])
-
-    def y_copy(zz, xx):
-        return remote(y_ref.at[zz, xx], got_ref.at[z, xx], ys.at[zz, xx], yr.at[z, xx], (g, zz, t))
-
-    def y_wait(zz, xx):
-        return remote(got_ref.at[zz, xx], got_ref.at[zz, xx], ys.at[zz, xx], yr.at[zz, xx], (g, z, t_x))
-
-    def others(act):
-        for d in range(n - 1, 0, -1):
-            pl.when(z - d >= 0)(functools.partial(act, z - d))
-            pl.when(z + d < n)(functools.partial(act, z + d))
-
-    for xx in (1 - x, x):
-        others(lambda zz: y_copy(zz, xx).start())
-    got_ref[z] = y_ref[z]
-    for copy in loads:
-        copy.wait()
-
-    def product(j, xx):
-        total = jnp.zeros((local, wide), f32)
-        at = pl.ds(pl.multiple_of(j * wide, wide), wide)
-        for zz in range(n):
-            total = total + jnp.dot(got_ref[zz, xx], p_ref[zz, :, at], preferred_element_type=f32)
-        return total
-
-    def d_copy(j):
-        return remote(away_ref.at[j], theirs_ref.at[j], ds.at[j], dr.at[j], (g, z, t_x))
-
-    others(lambda zz: y_wait(zz, 1 - x).wait_recv())
-
-    def send(j, carry):
-        value = product(j, 1 - x).astype(bf16)
-
-        @pl.when(j > 0)
-        def _():
-            d_copy(j - 1).start()
-
-        away_ref[j] = value
-        return carry
-
-    lax.fori_loop(0, steps, send, 0)
-    others(lambda zz: y_wait(zz, x).wait_recv())
-    d_copy(steps - 1).start()
-
-    def keep(j, carry):
-        mine_ref[j] = product(j, x)
-        return carry
-
-    lax.fori_loop(0, steps, keep, 0)
-    for j in range(steps):
-        d_copy(j).wait_recv()
-        out_ref[:, j * wide:(j + 1) * wide] = (mine_ref[j] + theirs_ref[j].astype(f32)).astype(bf16)
-    for j in range(steps):
-        d_copy(j).wait_send()
-    for xx in (1 - x, x):
-        others(lambda zz: y_copy(zz, xx).wait_send())
-
-
-def finish(n, y, proj_diff, proj_win, other_diff, other_win):
-    local, feats = y.shape[2:]
-    width = proj_diff.shape[1]
-    steps = 8
-    dma = pltpu.SemaphoreType.DMA
-    whole = pl.BlockSpec(memory_space=pltpu.VMEM)
-    far = pl.BlockSpec(memory_space=pl.ANY)
-    return pl.pallas_call(
-        functools.partial(finish_kernel, n),
-        in_specs=[whole] + [far] * 4,
-        out_specs=whole,
-        out_shape=jax.ShapeDtypeStruct((local, width), jnp.bfloat16),
-        scratch_shapes=[
-            pltpu.VMEM(y.shape, jnp.bfloat16),
-            pltpu.VMEM((n, feats, width), jnp.bfloat16),
-            pltpu.VMEM((steps, local, width // steps), jnp.float32),
-            pltpu.VMEM((steps, local, width // steps), jnp.bfloat16),
-            pltpu.VMEM((steps, local, width // steps), jnp.bfloat16),
-            dma((n, 2)), dma((n, 2)), dma((n // 2, 2, 2)), dma((steps,)), dma((steps,)),
-        ],
-        compiler_params=pltpu.CompilerParams(
-            collective_id=1, has_side_effects=True, vmem_limit_bytes=52 << 20
-        ),
-        cost_estimate=pl.CostEstimate(
-            flops=2 * 2 * local * n * feats * width, bytes_accessed=2 * n * feats * width, transcendentals=0
-        ),
-    )(y, proj_diff, proj_win, other_diff, other_win)
+    )(
+        tokens, norm_gain.reshape(1, width), query_diff, query_win, key_diff, value_diff, keyval_win,
+        proj_diff, proj_win, scal, output_norm_gain.reshape(1, VDIM),
+    )
 
 
 def split_body(
@@ -781,11 +758,10 @@
     n = lax.axis_size("sp")
     scal = jnp.stack([jnp.pad(lam, (0, LANES - lam.shape[0])), jnp.pad(sink, (0, LANES - sink.shape[0]))])
     scal = jnp.pad(scal, ((0, 6), (0, 0)))
-    res, other_diff, other_win, both = project(
-        n, tokens, norm_gain, query_diff, query_win, key_diff, value_diff, keyval_win, proj_diff, proj_win, scal
+    return whole(
+        n, tokens, norm_gain, query_diff, query_win, key_diff, value_diff, keyval_win, proj_diff, proj_win, scal,
+        output_norm_gain,
     )
-    y = attend(n, both, res, output_norm_gain)
-    return finish(n, y, proj_diff, proj_win, other_diff, other_win)
 
 
 def splits(mesh, tokens, query_diff, query_win, lam, sink):

time: 206 us -> 183 us (0.89); the launches traced: 204 us -> 183 us
  Pallas kernels: 199 us -> 180 us
    pallas_call x3 -> x1, Pallas kernels: 199 us -> 180 us  [whole(): pl.pallas_call(functools.partial(whole_kernel, n, held), in_specs=[inside...]
where the time goes in v2:
time: 183 us
  Pallas kernels  180 us (98%)
  local copies, waits for them, and re-layouts  2.96 us (2%)
    pallas_call x1, Pallas kernels, whole(): pl.pallas_call(functools.partial(whole_kernel, n, held), in_specs=[inside...  180 us

profile of v2, /device:TPU:9, one launch (start us, length us, event | category | flops | bytes accessed | tf_op | source)
XLA Modules:
  0.0 183.3 jit_solution(9573884853631691153)
XLA Ops:
  0.0 0.7 pad_bitcast_fusion
  0.7 0.6 select_maximum_fusion.scal_ref
  1.3 179.7 %shard_map.118 = bf16[128,4096]{1,0:T(8,128)(2,1)} custom-call(bf16[128,4096]{1,0:T(8,128)(2,1)} %tok_ref.1, f32[1,4096]{1,0:T(1,128)} %bitcast.6, bf16[1024,512]{1,0:T(8,128)(2,1)} %qd.1, bf16[1024,512]{1,0:T(8,128)(2,1)} %qw.1, bf16[1024,512]{1,0:T(8,128)(2,1)} %kd.1, bf16[1024,512]{1,0:T(8,128)(2,1)} %vd.1, bf16[4,1024,256]{2,1,0:T(8,128)(2,1)} %kvw.1, ...), custom_call_target="tpu_custom_call" | custom-call | flops 10737418240 | bytes 22020096 | tf_op jit(solution)/shard_map/pallas_call | solution.py:715
  181.0 2.3 %copy.14 = bf16[128,4096]{1,0:T(8,128)(2,1)} copy(bf16[128,4096]{1,0:T(8,128)(2,1)} %shard_map.118) | data formatting | bytes 2097152

commit v3 on v2

--- a/solution.py
+++ b/solution.py
@@ -252,10 +252,11 @@
     return g, z, t, x, c, 2 * (1 - x) + c, 2 * x + 1 - c
 
 
-def greet(devices):
+def greet(devices, meanwhile):
     barrier = pltpu.get_barrier_semaphore()
     for device in devices:
         pl.semaphore_signal(barrier, inc=1, device_id=device, device_id_type=MESH)
+    meanwhile()
     pl.semaphore_wait(barrier, len(devices))
 
 
@@ -285,13 +286,13 @@
 
 
 def whole_kernel(
-    n, held, tok_ref, gain_ref, qd, qw, kd, vd, kvw, pd, pw, scal_ref, out_gain_ref,
+    n, held, tok_hbm, gain_hbm, qd, qw, kd, vd, kvw, pd, pw, lam_ref, sink_ref, out_gain_ref,
     out_ref,
-    rows_ref, w_ref, sum_ref, res_ref, oscal_ref, p_ref, v_ref, y_ref, got_ref, mine_ref, away_ref, theirs_ref,
+    tok_ref, gain_ref, scal_ref, enter, rows_ref, w_ref, sum_ref, res_ref, oscal_ref, p_ref, v_ref, y_ref, got_ref, mine_ref, away_ref, theirs_ref,
     zs, zr, xs, xr, cs, cr, ws, wr, ys, yr, own_sem, rs, rr, ps, pr, load, scal_s, scal_r, hs, hr, ds, dr,
 ):
     g, z, t, x, c, t_x, t_c = place()
-    local, width = tok_ref.shape
+    local, width = tok_hbm.shape
     part = local // CHUNKS
     depth = qd.shape[0]
     half = depth // 2
@@ -303,15 +304,26 @@
     def block(zz, h, tt):
         return rows_ref.at[zz, h, pl.ds(pl.multiple_of(tt * part, part), part)]
 
-    for h in range(CHUNKS):
-        v = tok_ref[h * part:(h + 1) * part, :].astype(f32)
-        v = v * lax.rsqrt(jnp.mean(v * v, axis=-1, keepdims=True) + EPS) * gain_ref[...]
-        rows_ref[z, h, pl.ds(pl.multiple_of(t * part, part), part), :] = v.astype(bf16)
-    oscal_ref[c] = scal_ref[...]
+    entries = [pltpu.make_async_copy(tok_hbm, tok_ref, enter.at[0]), pltpu.make_async_copy(gain_hbm, gain_ref, enter.at[1])]
+    for copy in entries:
+        copy.start()
+
+    def normalize():
+        scal_ref[...] = jnp.zeros(scal_ref.shape, f32)
+        scal_ref[0:1, 0:held] = lam_ref[...]
+        scal_ref[1:2, 0:2 * held] = sink_ref[...]
+        oscal_ref[c] = scal_ref[...]
+        for copy in entries:
+            copy.wait()
+        for h in range(CHUNKS):
+            v = tok_ref[h * part:(h + 1) * part, :].astype(f32)
+            v = v * lax.rsqrt(jnp.mean(v * v, axis=-1, keepdims=True) + EPS) * gain_ref[...]
+            rows_ref[z, h, pl.ds(pl.multiple_of(t * part, part), part), :] = v.astype(bf16)
 
     greet(
         [(g, lax.rem(z + i // 2, n), 2 * x + (c + i % 2) % 2) for i in range(1, 2 * n)]
-        + [(g, z, t_x), (1 - g, z, t)]
+        + [(g, z, t_x), (1 - g, z, t)],
+        normalize,
     )
 
     def w_half(zz, yy, m):
@@ -533,7 +545,7 @@
 
     lam = scalar(0, z % held)
     sinks = [scalar(1, 2 * (z % held) + i) for i in range(2)]
-    first = lax.broadcasted_iota(jnp.int32, (2 * local, 1), 0) < local
+    first = lax.broadcasted_iota(jnp.int32, (local, 1), 0) < local // 2
     sink = jnp.where(first, sinks[0], sinks[1])
 
     distant = []
@@ -544,23 +556,29 @@
             zz = jnp.where(z == here, far, zz)
         distant.append(zz)
 
-    def pick(values, j):
-        value = values[0]
-        for i in range(1, len(values)):
-            value = jnp.where(j == i, values[i], value)
-        return value
-
-    def piece(i, zz, tt, m):
+    fine = local // 2
+    some = CHUNKS // 2
+
+    def piece(i, zz, tt, m, e=None):
         at = pl.ds(pl.multiple_of(tt * part, part), part)
-        return res_ref[i, zz, :, at, m * LANES:(m + 1) * LANES].reshape(local, LANES)
-
-    def y_copy_to(zz, xx):
-        return remote(y_ref.at[zz, xx], got_ref.at[z, xx], hs.at[zz, xx], hr.at[z, xx], (g, zz, t))
-
-    def y_wait(zz, xx):
-        return remote(got_ref.at[zz, xx], got_ref.at[zz, xx], hs.at[zz, xx], hr.at[zz, xx], (g, z, t_x))
-
-    def windowed(zz, tt, xx):
+        if e is None:
+            return res_ref[i, zz, :, at, m * LANES:(m + 1) * LANES].reshape(local, LANES)
+        return res_ref[i, zz, pl.ds(e * some, some), at, m * LANES:(m + 1) * LANES].reshape(fine, LANES)
+
+    def rows_of(e):
+        return pl.ds(pl.multiple_of(e * fine, fine), fine)
+
+    def y_copy_to(zz, xx, e):
+        return remote(
+            y_ref.at[zz, xx, rows_of(e)], got_ref.at[z, xx, rows_of(e)],
+            hs.at[zz, xx, e], hr.at[z, xx, e], (g, zz, t),
+        )
+
+    def y_wait(zz, xx, e):
+        rows = got_ref.at[zz, xx, rows_of(e)]
+        return remote(rows, rows, hs.at[zz, xx, e], hr.at[zz, xx, e], (g, z, t_x))
+
+    def windowed(zz, tt, xx, e):
         b = 4 * zz + tt
 
         def banded(i):
@@ -570,11 +588,11 @@
                 pieces.append(piece(i, o // 4, o % 4, 4))
             return jnp.concatenate(pieces, axis=0)
 
-        q = jnp.concatenate([piece(i, zz, tt, 1) for i in range(2)], axis=0)
+        q = jnp.concatenate([piece(i, zz, tt, 1, e) for i in range(2)], axis=0)
         scores = lax.dot_general(
             q, banded(0), (((1,), (1,)), ((), ())), preferred_element_type=f32
         ) * HEAD ** (-0.5)
-        r_index = lax.broadcasted_iota(jnp.int32, scores.shape, 0) % local
+        r_index = lax.broadcasted_iota(jnp.int32, scores.shape, 0) % fine + e * fine
         k_index = lax.broadcasted_iota(jnp.int32, scores.shape, 1)
         spot = (b - 1) * local + k_index
         valid = (jnp.abs(k_index - local - r_index) <= WINDOW) & (spot >= 0) & (spot < rows)
@@ -584,17 +602,15 @@
         weights = expo / (jnp.sum(expo, axis=-1, keepdims=True) + jnp.exp(sink - top))
         out = jnp.dot(weights.astype(bf16), banded(1), preferred_element_type=f32).astype(bf16)
         for i in range(2):
-            y_ref[zz, xx, :, VDIM + i * LANES:VDIM + (i + 1) * LANES] = out[i * local:(i + 1) * local]
-
-    def attend(step, carry):
-        pairs = n // 2
-        xx = jnp.where(step < pairs, 1 - x, x)
+            y_ref[zz, xx, rows_of(e), VDIM + i * LANES:VDIM + (i + 1) * LANES] = out[i * fine:(i + 1) * fine]
+
+    def attend(step):
+        xx = jnp.where(step < 2, 1 - x, x)
         tt = 2 * xx + c
-        j = step % pairs
-        zzs = [pick(distant[i::2], j) for i in range(2)]
+        e = step % 2
         maps = []
         for m in range(2):
-            q = jnp.concatenate([piece(m, zz, tt, 0) for zz in zzs], axis=0)
+            q = jnp.concatenate([piece(m, zz, tt, 0, e) for zz in distant], axis=0)
             keys = res_ref[m, :, :, :, 2 * LANES:3 * LANES].reshape(rows, LANES)
             scores = lax.dot_general(q, keys, (((1,), (1,)), ((), ())), preferred_element_type=f32)
             top = jnp.max(scores, axis=-1, keepdims=True)
@@ -605,22 +621,17 @@
         d = maps[0] - lam * maps[1]
         d = d * lax.rsqrt(jnp.mean(d * d, axis=-1, keepdims=True) + EPS) * out_gain_ref[...]
         d = d.astype(bf16)
-        for i, zz in enumerate(zzs):
-            y_ref[zz, xx, :, :VDIM] = d[i * local:(i + 1) * local]
-        for zz in zzs:
-            windowed(zz, tt, xx)
-        for zz in zzs:
+        for i, zz in enumerate(distant):
+            y_ref[zz, xx, rows_of(e), :VDIM] = d[i * fine:(i + 1) * fine]
+        for zz in distant:
+            windowed(zz, tt, xx, e)
+        for zz in distant:
             @pl.when(zz != z)
             def _():
-                y_copy_to(zz, xx).start()
-        return carry
-
-    lax.fori_loop(0, n, attend, 0)
-    got_ref[z] = y_ref[z]
-    for copy in loads + proj_copies:
-        copy.wait()
-
-    steps = mine_ref.shape[0]
+                y_copy_to(zz, xx, e).start()
+        got_ref[z, xx, rows_of(e)] = y_ref[z, xx, rows_of(e)]
+
+    steps = mine_ref.shape[1]
     wide = width // steps
 
     def others(act):
@@ -628,44 +639,67 @@
             pl.when(z - d >= 0)(functools.partial(act, z - d))
             pl.when(z + d < n)(functools.partial(act, z + d))
 
-    def product(j, xx):
-        total = jnp.zeros((local, wide), f32)
+    def product(j, xx, e):
+        total = jnp.zeros((fine, wide), f32)
         at = pl.ds(pl.multiple_of(j * wide, wide), wide)
         for zz in range(n):
-            total = total + jnp.dot(got_ref[zz, xx], p_ref[zz, :, at], preferred_element_type=f32)
+            total = total + jnp.dot(
+                got_ref[zz, xx, rows_of(e)], p_ref[zz, :, at], preferred_element_type=f32
+            )
         return total
 
-    def d_copy(j):
-        return remote(away_ref.at[j], theirs_ref.at[j], ds.at[j], dr.at[j], (g, z, t_x))
-
-    others(lambda zz: y_wait(zz, 1 - x).wait_recv())
-
-    def send(j, carry):
-        value = product(j, 1 - x).astype(bf16)
-
-        @pl.when(j > 0)
+    def d_copy(e, j):
+        return remote(away_ref.at[e, j], theirs_ref.at[e, j], ds.at[e, j], dr.at[e, j], (g, z, t_x))
+
+    def send_rows(e):
+        @pl.when(e == 0)
         def _():
-            d_copy(j - 1).start()
-
-        away_ref[j] = value
+            for copy in loads + proj_copies:
+                copy.wait()
+
+        others(lambda zz: y_wait(zz, 1 - x, e).wait_recv())
+
+        def send(j, carry):
+            value = product(j, 1 - x, e).astype(bf16)
+
+            @pl.when(j > 0)
+            def _():
+                d_copy(e, j - 1).start()
+
+            away_ref[e, j] = value
+            return carry
+
+        lax.fori_loop(0, steps, send, 0)
+        d_copy(e, steps - 1).start()
+
+    def stage(step, carry):
+        attend(step)
+        pl.when((step >= 1) & (step <= 2))(lambda: send_rows(step - 1))
         return carry
 
-    lax.fori_loop(0, steps, send, 0)
-    others(lambda zz: y_wait(zz, x).wait_recv())
-    d_copy(steps - 1).start()
-
-    def keep(j, carry):
-        mine_ref[j] = product(j, x)
+    lax.fori_loop(0, 4, stage, 0)
+
+    def keep_rows(e, carry):
+        others(lambda zz: y_wait(zz, x, e).wait_recv())
+
+        def keep(j, carry):
+            mine_ref[e, j] = product(j, x, e)
+            return carry
+
+        lax.fori_loop(0, steps, keep, 0)
         return carry
 
-    lax.fori_loop(0, steps, keep, 0)
-    for j in range(steps):
-        d_copy(j).wait_recv()
-        out_ref[:, j * wide:(j + 1) * wide] = (mine_ref[j] + theirs_ref[j].astype(f32)).astype(bf16)
-    for j in range(steps):
-        d_copy(j).wait_send()
-    for xx in (1 - x, x):
-        others(lambda zz: y_copy_to(zz, xx).wait_send())
+    lax.fori_loop(0, 2, keep_rows, 0)
+    for e in range(2):
+        for j in range(steps):
+            d_copy(e, j).wait_recv()
+            total = mine_ref[e, j] + theirs_ref[e, j].astype(f32)
+            out_ref[e * fine:(e + 1) * fine, j * wide:(j + 1) * wide] = total.astype(bf16)
+    for e in range(2):
+        for j in range(steps):
+            d_copy(e, j).wait_send()
+        for xx in (1 - x, x):
+            others(lambda zz: y_copy_to(zz, xx, e).wait_send())
 
     def drain(here):
         for way in range(2):
@@ -698,7 +732,7 @@
 
 
 def whole(
-    n, tokens, norm_gain, query_diff, query_win, key_diff, value_diff, keyval_win, proj_diff, proj_win, scal,
+    n, tokens, norm_gain, query_diff, query_win, key_diff, value_diff, keyval_win, proj_diff, proj_win, lam, sink,
     output_norm_gain,
 ):
     local, width = tokens.shape
@@ -709,27 +743,31 @@
     cols = MATS * LANES
     tok = 4 * local * n
     feats = VDIM + 2 * HEAD
-    steps = 8
+    steps = 4
     quad = 4 * local // CHUNKS
     bf16, f32 = jnp.bfloat16, jnp.float32
     return pl.pallas_call(
         functools.partial(whole_kernel, n, held),
-        in_specs=[inside, inside] + [far] * 7 + [inside, inside],
+        in_specs=[far] * 9 + [inside] * 3,
         out_specs=inside,
         out_shape=jax.ShapeDtypeStruct((local, width), bf16),
         scratch_shapes=[
+            pltpu.VMEM((local, width), bf16),
+            pltpu.VMEM((1, width), f32),
+            pltpu.VMEM((8, LANES), f32),
+            dma((2,)),
             pltpu.VMEM((n, CHUNKS, quad, width), bf16),
             pltpu.VMEM((width, cols), bf16),
             pltpu.VMEM((n, 4 * local, cols), f32),
             pltpu.VMEM((2, n, CHUNKS, quad, cols), bf16),
-            pltpu.VMEM((2,) + scal.shape, f32),
+            pltpu.VMEM((2, 8, LANES), f32),
             pltpu.VMEM((n, feats, width), bf16),
             pltpu.VMEM((tok, VDIM), bf16),
             pltpu.VMEM((n, 2, local, feats), bf16),
             pltpu.VMEM((n, 2, local, feats), bf16),
-            pltpu.VMEM((steps, local, width // steps), f32),
-            pltpu.VMEM((steps, local, width // steps), bf16),
-            pltpu.VMEM((steps, local, width // steps), bf16),
+            pltpu.VMEM((2, steps, local // 2, width // steps), f32),
+            pltpu.VMEM((2, steps, local // 2, width // steps), bf16),
+            pltpu.VMEM((2, steps, local // 2, width // steps), bf16),
             dma((2, n, CHUNKS)), dma((2, n + 1, CHUNKS)),
             dma((n, CHUNKS)), dma((n, CHUNKS)),
             dma((n, 2, CHUNKS)), dma((n, 2, CHUNKS)),
@@ -737,7 +775,7 @@
             dma((n, MATS)), dma((n, MATS)), dma((MATS,)),
             dma((n, 3)), dma((n, 3)),
             dma((held, 2)), dma((held, 2)), dma((held, 2)), dma, dma,
-            dma((n, 2)), dma((n, 2)), dma((steps,)), dma((steps,)),
+            dma((n, 2, 2)), dma((n, 2, 2)), dma((2, steps)), dma((2, steps)),
         ],
         compiler_params=pltpu.CompilerParams(
             collective_id=0, has_side_effects=True, vmem_limit_bytes=67043328
@@ -747,7 +785,7 @@
         ),
     )(
         tokens, norm_gain.reshape(1, width), query_diff, query_win, key_diff, value_diff, keyval_win,
-        proj_diff, proj_win, scal, output_norm_gain.reshape(1, VDIM),
+        proj_diff, proj_win, lam.reshape(1, -1), sink.reshape(1, -1), output_norm_gain.reshape(1, VDIM),
     )
 
 
@@ -756,10 +794,8 @@
     query_win, keyval_win, sink, proj_diff, proj_win,
 ):
     n = lax.axis_size("sp")
-    scal = jnp.stack([jnp.pad(lam, (0, LANES - lam.shape[0])), jnp.pad(sink, (0, LANES - sink.shape[0]))])
-    scal = jnp.pad(scal, ((0, 6), (0, 0)))
     return whole(
-        n, tokens, norm_gain, query_diff, query_win, key_diff, value_diff, keyval_win, proj_diff, proj_win, scal,
+        n, tokens, norm_gain, query_diff, query_win, key_diff, value_diff, keyval_win, proj_diff, proj_win, lam, sink,
         output_norm_gain,
     )
 

time: 183 us -> 179 us (0.978)
  Pallas kernels: 180 us -> 176 us
    pallas_call x1, Pallas kernels: 180 us -> 176 us  [whole(): pl.pallas_call(functools.partial(whole_kernel, n, held), in_specs=[far] *...]
where the time goes in v3:
time: 179 us; the launch traced here: 178 us
  Pallas kernels  176 us (98%)
  local copies, waits for them, and re-layouts  2.29 us (1%)
    pallas_call x1, Pallas kernels, whole(): pl.pallas_call(functools.partial(whole_kernel, n, held), in_specs=[far] *...  176 us

profile of v3, /device:TPU:9, one launch (start us, length us, event | category | flops | bytes accessed | tf_op | source)
XLA Modules:
  0.0 178.3 jit_solution(7924577430896941991)
XLA Ops:
  0.0 176.0 %shard_map.118 = bf16[128,4096]{1,0:T(8,128)(2,1)} custom-call(bf16[128,4096]{1,0:T(8,128)(2,1)} %tok_hbm.1, f32[1,4096]{1,0:T(1,128)} %bitcast.4, bf16[1024,512]{1,0:T(8,128)(2,1)} %qd.1, bf16[1024,512]{1,0:T(8,128)(2,1)} %qw.1, bf16[1024,512]{1,0:T(8,128)(2,1)} %kd.1, bf16[1024,512]{1,0:T(8,128)(2,1)} %vd.1, bf16[4,1024,256]{2,1,0:T(8,128)(2,1)} %kvw.1, ...), custom_call_target="tpu_custom_call" | custom-call | flops 10737418240 | bytes 22020096 | tf_op jit(solution)/shard_map/pallas_call | solution.py:749
  176.1 2.3 %copy.14 = bf16[128,4096]{1,0:T(8,128)(2,1)} copy(bf16[128,4096]{1,0:T(8,128)(2,1)} %shard_map.118) | data formatting | bytes 2097152

commit v4 on v3

--- a/solution.py
+++ b/solution.py
@@ -347,7 +347,7 @@
             @pl.when(c == cs_)
             def _():
                 for m in range(MATS):
-                    for dz in range(cs_ * held, (cs_ + 1) * held):
+                    for dz in sorted(range(cs_ * held, (cs_ + 1) * held), key=lambda o: abs(o - here)):
                         if (dz > here) if way == 0 else (dz < here):
                             for cc in range(2):
                                 act(w_copy(here, dz, cc, m))
@@ -395,6 +395,14 @@
             remote(w_half(zz, 1 - g, m), w_half(zz, 1 - g, m), ys.at[zz, m], yr.at[zz, m], core).wait_recv()
 
     scal_copy = remote(scal_ref, oscal_ref.at[c], scal_s, scal_r, core)
+
+    proj_copies, loads = [], []
+    for i in range(held):
+        for j, ref in enumerate((pd, pw)):
+            rows = ref.at[i * VDIM:(i + 1) * VDIM]
+            at = p_ref.at[c * held + i, j * VDIM:(j + 1) * VDIM]
+            loads.append(pltpu.make_async_copy(rows, at, load.at[i, j]))
+            proj_copies.append(remote(rows, at, ps.at[i, j], pr.at[i, j], core))
 
     def gather(here):
         for h in range(CHUNKS):
@@ -405,6 +413,8 @@
             x_copy(here, h).start()
             c_copy(here, x, h).start()
         scal_copy.start()
+        for copy in loads + proj_copies:
+            copy.start()
         own_each(here, lambda copy: copy.start(), lambda copy: copy.start())
         if here == 0:
             w_each(here, 0, lambda copy: copy.start())
@@ -432,15 +442,6 @@
     for here in range(n):
         pl.when(z == here)(functools.partial(gather, here))
 
-    proj_copies, loads = [], []
-    for i in range(held):
-        for j, ref in enumerate((pd, pw)):
-            rows = ref.at[i * VDIM:(i + 1) * VDIM]
-            at = p_ref.at[c * held + i, j * VDIM:(j + 1) * VDIM]
-            loads.append(pltpu.make_async_copy(rows, at, load.at[i, j]))
-            proj_copies.append(remote(rows, at, ps.at[i, j], pr.at[i, j], core))
-    for copy in loads + proj_copies:
-        copy.start()
 
     sources = []
     for j in range(n - 1):
@@ -493,13 +494,13 @@
             for zz in late:
                 forward(zz, m)
 
-    forwards(0, 1)
+    forwards(0, 2)
     lax.fori_loop(0, n, opening, 0)
-    forwards(1, 2)
+    forwards(2, 3)
     add(sources[0] * depth + g * half)
     crossed(sources[0])
     add(sources[0] * depth + (1 - g) * half)
-    forwards(2, MATS)
+    forwards(3, MATS)
     for zz in late:
         add(zz * depth + g * half)
     for zz in late[:-1]:

time: 179 us -> 176 us (0.983)
  Pallas kernels: 176 us -> 173 us
    pallas_call x1, Pallas kernels: 176 us -> 173 us  [whole(): pl.pallas_call(functools.partial(whole_kernel, n, held), in_specs=[far] *...]
where the time goes in v4:
time: 176 us
  Pallas kernels  173 us (98%)
  local copies, waits for them, and re-layouts  2.29 us (1%)
    pallas_call x1, Pallas kernels, whole(): pl.pallas_call(functools.partial(whole_kernel, n, held), in_specs=[far] *...  173 us

profile of v4, /device:TPU:9, one launch (start us, length us, event | category | flops | bytes accessed | tf_op | source)
XLA Modules:
  0.0 175.6 jit_solution(15416539245008903042)
XLA Ops:
  0.0 173.3 %shard_map.118 = bf16[128,4096]{1,0:T(8,128)(2,1)} custom-call(bf16[128,4096]{1,0:T(8,128)(2,1)} %tok_hbm.1, f32[1,4096]{1,0:T(1,128)} %bitcast.4, bf16[1024,512]{1,0:T(8,128)(2,1)} %qd.1, bf16[1024,512]{1,0:T(8,128)(2,1)} %qw.1, bf16[1024,512]{1,0:T(8,128)(2,1)} %kd.1, bf16[1024,512]{1,0:T(8,128)(2,1)} %vd.1, bf16[4,1024,256]{2,1,0:T(8,128)(2,1)} %kvw.1, ...), custom_call_target="tpu_custom_call" | custom-call | flops 10737418240 | bytes 22020096 | tf_op jit(solution)/shard_map/pallas_call | solution.py:750
  173.3 2.3 %copy.14 = bf16[128,4096]{1,0:T(8,128)(2,1)} copy(bf16[128,4096]{1,0:T(8,128)(2,1)} %shard_map.118) | data formatting | bytes 2097152
